TPU v7x, 512 devices: a whole 4x8x8 slice. The times are simulated.
512 devices in a mesh: ep: 128 (over z, y, core), tp: 4 (over x).
Axes of the slice: x: 4, y: 8, z: 8, core: 2. Of those that a mesh axis runs over, the one named last changes fastest.
Arguments:
- tokens: bfloat16 [2048, 1024], P(('ep', 'tp')), may hold values from -6 to 6
- gain_attn: bfloat16 [1024], replicated, may hold values from 0.099609375 to 1.8984375
- gain_ffn: bfloat16 [1024], replicated, may hold values from 0.099609375 to 1.8984375
- w_query: bfloat16 [1024, 512], P(None, 'tp'), may hold values from -0.1875 to 0.1875
- w_key: bfloat16 [1024, 128], replicated, may hold values from -0.1875 to 0.1875
- w_value: bfloat16 [1024, 128], replicated, may hold values from -0.1875 to 0.1875
- w_output: bfloat16 [512, 1024], P('tp'), may hold values from -0.25 to 0.25
- head_bias: float32 [8], replicated, may hold values from -9 to -2
- keys_cache: bfloat16 [2048, 1024, 128], P(('ep', 'tp')), may hold values from -6 to 6
- values_cache: bfloat16 [2048, 1024, 128], P(('ep', 'tp')), may hold values from -6 to 6
- lengths: int32 [2048], P(('ep', 'tp')), may hold values from 256 to 1024
- dense_gate_w: bfloat16 [4096, 1024], P('ep'), may hold values from -0.1875 to 0.1875
- dense_up_w: bfloat16 [4096, 1024], P('ep'), may hold values from -0.1875 to 0.1875
- dense_down_w: bfloat16 [4096, 1024], P('ep'), may hold values from -0.09375 to 0.09375
- mix_gate: bfloat16 [1024], replicated, may hold values from -0.1875 to 0.1875
- expert_gate: bfloat16 [128, 1024, 1024], P('ep', None, 'tp'), may hold values from -0.1875 to 0.1875
- expert_up: bfloat16 [128, 1024, 1024], P('ep', None, 'tp'), may hold values from -0.1875 to 0.1875
- expert_down: bfloat16 [128, 1024, 1024], P('ep', 'tp'), may hold values from -0.09375 to 0.09375
- routes: int32 [2048, 2], P(('ep', 'tp')), may hold values from 0 to 31, all different within a row; in each aligned block of 16 rows (0 to 15, 16 to 31, ...) at most 2 rows name the same one
- route_weights: float32 [2048, 2], P(('ep', 'tp')), may hold values from 0.1 to 0.9
Outputs:
- layer_out: bfloat16 [2048, 1024], P(('ep', 'tp'))
- new_keys: bfloat16 [2048, 128], P(('ep', 'tp'))
- new_values: bfloat16 [2048, 128], P(('ep', 'tp'))
Inputs may be any that keep to these rules, and one draw needn't show every extreme that they name: `routes`: each row names 2 different experts. In each aligned block of 16 rows (the tokens held by one index of ep) no expert is named by more than 2 rows, a bound that some block reaches.
All inputs are finite; a program needn't handle non-finite values.
Results may differ from a plain program's by a relative error of at most 0.01.
Values may be sent and summed in bfloat16 or wider, within the bound.
No kernel may reach another device: no remote copies, remote signals or barrier semaphores. Data moves between devices by JAX's collectives and lax.ppermute only.
A program may use at most 64 MiB of HBM per device.

v0:
```python
import math

import jax
import jax.numpy as jnp
from jax import lax
from jax.experimental import pallas as pl
from jax.experimental.pallas import tpu as pltpu
from jax.sharding import Mesh, PartitionSpec as P


HEADS = 8
KV = 2
HEAD = 64
EPS = 1e-06
D = 1024
HALF = D // 2
CACHE = 1024
OWN = 4
TP = 4
CHIPS = 64
MSG = 8
ROWS = CHIPS * MSG
F32 = jnp.float32
BF16 = jnp.bfloat16


VMEM = pl.BlockSpec(memory_space=pltpu.VMEM)
SMEM = pl.BlockSpec(memory_space=pltpu.SMEM)
HBM = pl.BlockSpec(memory_space=pltpu.HBM)
EXPERT_ROWS = 3 * D
DENSE_ROWS = 96
SIB_SCRATCH = [
    pltpu.VMEM((EXPERT_ROWS + 8 * DENSE_ROWS, 256), jnp.bfloat16),
    pltpu.SemaphoreType.DMA((7,)),
]


def dot(a, b):
    return lax.dot_general(a, b, (((1,), (0,)), ((), ())), preferred_element_type=F32)


def dot_t(a, b):
    return lax.dot_general(a, b, (((1,), (1,)), ((), ())), preferred_element_type=F32)


def iota(shape, dim):
    return lax.broadcasted_iota(jnp.int32, shape, dim)


def call(kernel, out_shape, specs, scratch=(), limit=4):
    outs = jax.tree.map(lambda _: VMEM, out_shape)
    return pl.pallas_call(
        kernel,
        out_shape=out_shape,
        in_specs=specs,
        out_specs=outs,
        scratch_shapes=list(scratch),
        compiler_params=pltpu.CompilerParams(vmem_limit_bytes=limit * 1024 * 1024),
    )


def rms(values, gains):
    wide = values.astype(F32)
    scale = lax.rsqrt(jnp.mean(wide * wide, axis=-1, keepdims=True) + EPS)
    return (wide * scale) * gains.astype(F32)


def pack_kernel(core, wq, wo, routes_hbm, weights_hbm, gate, up, down, out, dense, routes, weights, sems):
    start = core[0] * HALF
    facts = [
        pltpu.make_async_copy(routes_hbm, routes, sems.at[8]),
        pltpu.make_async_copy(weights_hbm, weights, sems.at[9]),
    ]
    for c in facts:
        c.start()
    copies = [
        pltpu.make_async_copy(
            wq.at[pl.ds(pl.multiple_of(start, HALF), HALF), :], out.at[0, 0:HALF, :], sems.at[0]
        )
    ]
    for j in range(4):
        copies.append(
            pltpu.make_async_copy(
                wo.at[:, pl.ds(pl.multiple_of(start + j * 128, 128), 128)],
                out.at[0, HALF + 128 * j : HALF + 128 * (j + 1), :],
                sems.at[1 + j],
            )
        )
    for k, ref in enumerate((gate, up, down)):
        copies.append(
            pltpu.make_async_copy(ref, dense.at[32 * k : 32 * (k + 1), :], sems.at[5 + k])
        )
    for c in copies:
        c.start()
    for c in facts:
        c.wait()
    eye = iota((OWN, OWN), 0) == iota((OWN, OWN), 1)

    def column(row):
        return jnp.sum(jnp.where(eye, row, 0.0), axis=1, keepdims=True)

    ids, wts = routes[...].astype(F32), weights[...]
    high = wts.astype(BF16).astype(F32)
    low = wts - high
    lane = iota((OWN, 128), 1)
    info = jnp.zeros((OWN, 128), F32)
    for place, row in enumerate((ids[0:1], ids[1:2], high[0:1], low[0:1], high[1:2], low[1:2])):
        info = jnp.where(lane == place, column(row), info)
    info = jnp.concatenate([info, info], axis=0).astype(BF16)
    for d in range(TP):
        out[d, 2 * HALF : 2 * HALF + 8, :] = info
    for c in copies:
        c.wait()
    for d in range(1, TP):
        out[d, 0 : 2 * HALF, :] = out[0, 0 : 2 * HALF, :]


def norm_kernel(tokens, gain, wk, wv, attn_in, new_k, new_v):
    a = rms(tokens[...], gain[...]).astype(BF16)
    attn_in[...] = a
    new_k[...] = dot(a, wk[...]).astype(BF16)
    new_v[...] = dot(a, wv[...]).astype(BF16)


def expert_pack_kernel(gate, up, down, dense_own, dense_y, out):
    out[0:D, :] = gate[...]
    out[D : 2 * D, :] = up[...]
    base = 2 * D
    for ref in (down, dense_own, dense_y):
        n = ref.shape[0]
        for j in range(4):
            out[base : base + n, :] = ref[:, 256 * j : 256 * (j + 1)]
            base = base + n


def attend_kernel(
    core, lengths, tokens, attn_in, w_own, w_sib, bias, keys, values, gain, residual, sent
):
    first = core[0] == 0

    def ordered(a, b):
        return jnp.where(first, a, b)

    a = attn_in[...].astype(F32)
    x_own = ordered(a[:, :HALF], a[:, HALF:]).astype(BF16)
    x_sib = ordered(a[:, HALF:], a[:, :HALF]).astype(BF16)
    q = jnp.concatenate(
        [dot(x_own, w_own[t, 0:HALF, :]) + dot(x_sib, w_sib[t, 0:HALF, :]) for t in range(TP)],
        axis=1,
    )
    q = q.astype(BF16).astype(F32)
    head_mask = iota((HEADS, HEADS * HEAD), 1) // HEAD == iota((HEADS, HEADS * HEAD), 0)
    spread = jnp.concatenate(
        [
            jnp.where(head_mask, jnp.broadcast_to(q[b : b + 1], (HEADS, HEADS * HEAD)), 0.0)
            for b in range(OWN)
        ],
        axis=0,
    ).astype(BF16)
    source = iota((HEADS * HEAD, 128), 0)
    fold = (
        (source // (HEADS * HEAD // KV)) * HEAD + source % HEAD == iota((HEADS * HEAD, 128), 1)
    ).astype(F32)
    fold = fold.astype(BF16)
    q_blocks = dot(spread, fold).astype(BF16)
    position = iota((HEADS, CACHE), 1)
    eye = iota((HEADS, HEADS), 0) == iota((HEADS, HEADS), 1)
    offset = jnp.sum(jnp.where(eye, bias[...], 0.0), axis=1, keepdims=True)
    logs, skips, lives = [], [], []
    for b in range(OWN):
        s = dot_t(q_blocks[8 * b : 8 * b + 8], keys[b])
        s = s * (1.0 / math.sqrt(HEAD)) + offset
        tail = jnp.log1p(jnp.exp(-jnp.abs(s)))
        live = position < lengths[b]
        logs.append(jnp.minimum(s, 0.0) - tail)
        skips.append(jnp.where(live, jnp.minimum(-s, 0.0) - tail, 0.0))
        lives.append(live)
    chunks = CACHE // 128
    stacked = jnp.concatenate(
        [skips[b][:, 128 * k : 128 * k + 128] for b in range(OWN) for k in range(chunks)], axis=0
    )
    after = (iota((128, 128), 0) > iota((128, 128), 1)).astype(F32).astype(BF16)
    p1 = stacked.astype(BF16)
    rest = stacked - p1.astype(F32)
    p2 = rest.astype(BF16)
    p3 = (rest - p2.astype(F32)).astype(BF16)
    inner = dot(p1, after) + dot(p2, after) + dot(p3, after)
    totals = jnp.sum(stacked, axis=1, keepdims=True)
    mixes = []
    for b in range(OWN):
        carry = jnp.zeros((HEADS, 1), F32)
        later = [None] * chunks
        for k in reversed(range(chunks)):
            row = 8 * (b * chunks + k)
            later[k] = inner[row : row + 8] + carry
            carry = carry + totals[row : row + 8]
        later = jnp.concatenate(later, axis=1)
        weights = jnp.where(lives[b], jnp.exp(logs[b] + later), 0.0).astype(BF16)
        mixes.append(dot(weights, values[b]))
    mixed = jnp.concatenate(mixes, axis=0).astype(BF16)
    wide = dot_t(mixed, fold)
    mixed = jnp.concatenate(
        [
            jnp.sum(jnp.where(head_mask, wide[8 * b : 8 * b + 8], 0.0), axis=0, keepdims=True)
            for b in range(OWN)
        ],
        axis=0,
    ).astype(BF16)

    def project(w):
        parts = []
        for j in range(4):
            row = HALF + 128 * j
            acc = dot(mixed[:, 0:128], w[0, row : row + 128, :])
            for t in range(1, TP):
                acc = acc + dot(mixed[:, 128 * t : 128 * t + 128], w[t, row : row + 128, :])
            parts.append(acc)
        return jnp.concatenate(parts, axis=1)

    out_own, out_sib = project(w_own), project(w_sib)
    total = jnp.concatenate([ordered(out_own, out_sib), ordered(out_sib, out_own)], axis=1)
    res = (tokens[...].astype(F32) + total).astype(BF16)
    residual[...] = res
    f = rms(res, gain[...])
    f = jnp.concatenate([f[:, :HALF], f[:, HALF:]], axis=0).astype(BF16)
    for d in range(TP):
        sent[d] = f


def table_kernel(
    tp, own_hbm, keys_hbm, values_hbm, pick, weight, mine_out, own, keys, values, sems
):
    copies = [
        [pltpu.make_async_copy(src.at[b], dst.at[b], sems.at[k, b]) for b in range(OWN)]
        for k, (src, dst) in enumerate(((own_hbm, own), (keys_hbm, keys), (values_hbm, values)))
    ]
    for group in copies:
        for c in group:
            c.start()
    for c in copies[0]:
        c.wait()
    n = TP * 8
    row, col = iota((n, ROWS), 0), iota((n, ROWS), 1)
    facts = jnp.concatenate([own[t, 2 * HALF :, :] for t in range(TP)], axis=0).astype(F32)
    id0, id1 = facts[:, 0:1], facts[:, 1:2]
    w0, w1 = facts[:, 2:3] + facts[:, 3:4], facts[:, 4:5] + facts[:, 5:6]
    chip, r = col // MSG, col % 4
    expert = (chip // 2).astype(F32)
    is0, is1 = id0 == expert, id1 == expert
    chosen = jnp.where(is0 | is1, 1.0, 0.0)
    ra, rb = iota((n, n), 0), iota((n, n), 1)
    before = ((rb // 4) % 2 == 0) & (rb // 8 * 4 + rb % 4 < ra // 8 * 4 + ra % 4)
    earlier = dot(before.astype(F32).astype(BF16), chosen.astype(BF16))
    same_half = (row // 4) % 2 == (col // 4) % 2
    slot = same_half & (r < 2) & (chosen > 0.5) & (earlier == r.astype(F32))
    mine = same_half & (r >= 2) & (row // 8 == tp[0]) & (row % 4 == r - 2 + 2 * (chip % 2))
    pick[...] = jnp.where(slot | mine, 1.0, 0.0).T.astype(BF16)
    weight[...] = jnp.where(slot, jnp.where(is0, w0, w1), 0.0)
    mine_out[...] = jnp.where(mine, 1.0, 0.0)
    for group in copies[1:]:
        for c in group:
            c.wait()


def send_kernel(pick, group, sent):
    sent[...] = dot(pick[...], group[...]).astype(BF16)


def mix_kernel(group, mix_gate, mix):
    n = TP * 8
    first_half = (iota((n, 1), 0) // 4) % 2 == 0
    gates = mix_gate[...].astype(F32)
    gate_rows = jnp.where(first_half, gates[0:1, :], gates[1:2, :])
    part = jnp.sum(group[...].astype(F32) * gate_rows, axis=1, keepdims=True)
    part = jnp.broadcast_to(part, (n, 128))
    other = jnp.where(first_half, pltpu.roll(part, n - 4, 0), pltpu.roll(part, 4, 0))
    mix[...] = 1.0 / (1.0 + jnp.exp(-(part + other)))


def weigh_kernel(mix, weight, mine, combine):
    total = weight[...] + mine[...] * mix[:, 0:1]
    high = total.astype(BF16)
    combine[0] = high
    combine[1] = (total - high.astype(F32)).astype(BF16)


def expert_kernel(x, gate, up, down, sib_hbm, dense_own, dense_y, out, sib, sems):
    edges = [0, D // 2, D, 3 * D // 2, 2 * D, 5 * D // 2, EXPERT_ROWS, EXPERT_ROWS + 8 * DENSE_ROWS]
    copies = [
        pltpu.make_async_copy(sib_hbm.at[lo:hi, :], sib.at[lo:hi, :], sems.at[k])
        for k, (lo, hi) in enumerate(zip(edges[:-1], edges[1:]))
    ]
    for c in copies:
        c.start()
    rows = CHIPS * 4
    i, k = iota((rows, ROWS), 0), iota((rows, ROWS), 1)
    at = (i // 4) * MSG + i % 4
    halves = [(k == at + 4 * h).astype(F32).astype(BF16) for h in range(2)]
    got = x[...]
    xs = jnp.concatenate([dot(p, got) for p in halves], axis=1).astype(BF16)
    is_slot = iota((rows, 1), 0) % 4 < 2

    def hidden(g, u, keep):
        return jnp.where(keep, g / (1.0 + jnp.exp(-g)) * u, 0.0).astype(BF16)

    h_own = hidden(dot(xs, gate[...]), dot(xs, up[...]), is_slot)
    total = dot(h_own, down[...])
    for c in copies:
        c.wait()
    h_sib = hidden(dot(xs, sib[0:D, :]), dot(xs, sib[D : 2 * D, :]), is_slot)

    def stack(base):
        parts = [ref[base : base + 32, :] for ref in (dense_own, dense_y)]
        for k in range(2):
            first = EXPERT_ROWS + 4 * DENSE_ROWS * k + base
            parts.append(
                jnp.concatenate(
                    [sib[first + DENSE_ROWS * j : first + DENSE_ROWS * j + 32, :] for j in range(4)],
                    axis=1,
                )
            )
        return jnp.concatenate(parts, axis=0)

    h_dense = hidden(dot_t(xs, stack(0)), dot_t(xs, stack(32)), jnp.logical_not(is_slot))
    total = total + dot(h_dense, stack(64))
    total = total + jnp.concatenate(
        [dot(h_sib, sib[2 * D + 256 * j : 2 * D + 256 * (j + 1), :]) for j in range(4)], axis=1
    )
    total = total.astype(BF16)
    i, k = iota((ROWS, rows), 1), iota((ROWS, rows), 0)
    at = (i // 4) * MSG + i % 4
    res = None
    for h in range(2):
        p = (k == at + 4 * h).astype(F32).astype(BF16)
        part = dot(p, total[:, HALF * h : HALF * (h + 1)])
        res = part if res is None else res + part
    out[...] = res.astype(BF16)


def combine_kernel(combine, returned, out):
    got = returned[...]
    total = dot(combine[0], got) + dot(combine[1], got)
    out[...] = total.astype(BF16)


def finish_kernel(residual, parts, out):
    total = parts[0].astype(F32)
    for t in range(1, TP):
        total = total + parts[t].astype(F32)
    total = jnp.concatenate([total[0:4, :], total[4:8, :]], axis=1)
    out[...] = (residual[...].astype(F32) + total).astype(BF16)


def in_hbm(array):
    return pltpu.with_memory_space_constraint(array, pltpu.HBM)


def in_vmem(array):
    return pltpu.with_memory_space_constraint(array, pltpu.VMEM)


def shape(*dims, dtype=BF16):
    return jax.ShapeDtypeStruct(dims, dtype)


def a2a(array, axis):
    return lax.all_to_all(array, axis, split_axis=0, concat_axis=0, tiled=True)


def swap(array, axis):
    return lax.ppermute(array, axis, [(i, i ^ 1) for i in range(lax.axis_size(axis))])


def body(
    tokens,
    gain_attn,
    gain_ffn,
    w_query,
    w_key,
    w_value,
    w_output,
    head_bias,
    keys_cache,
    values_cache,
    lengths,
    dense_gate_w,
    dense_up_w,
    dense_down_w,
    mix_gate,
    expert_gate,
    expert_up,
    expert_down,
    routes,
    route_weights,
):
    core = lax.axis_index("c").astype(jnp.int32).reshape(1)
    tp = lax.axis_index("x").astype(jnp.int32).reshape(1)
    wlen = 2 * HALF + 8
    packed, dense_own = call(
        pack_kernel,
        (shape(TP, wlen, 128), shape(DENSE_ROWS, D)),
        [SMEM] + [HBM] * 7,
        [pltpu.VMEM((2, OWN), jnp.int32), pltpu.VMEM((2, OWN), F32), pltpu.SemaphoreType.DMA((10,))],
    )(
        core,
        in_hbm(w_query),
        in_hbm(w_output),
        in_hbm(routes.T),
        in_hbm(route_weights.T),
        in_hbm(dense_gate_w),
        in_hbm(dense_up_w),
        in_hbm(dense_down_w),
    )
    w_own = a2a(packed, "x")
    w_sib = swap(w_own, "c")
    dense_y = swap(dense_own, "y")
    expert_own = call(
        expert_pack_kernel, shape(EXPERT_ROWS + 8 * DENSE_ROWS, 256), [VMEM] * 5, limit=8
    )(expert_gate[0], expert_up[0], expert_down[0], dense_own, dense_y)
    expert_sib = swap(expert_own, "c")
    attn_in, new_keys, new_values = call(
        norm_kernel, (shape(OWN, D), shape(OWN, 128), shape(OWN, 128)), [VMEM] * 4
    )(tokens, gain_attn.reshape(1, D), w_key, w_value)
    cache = pltpu.VMEM((OWN, CACHE, 128), BF16)
    pick, weight, mine, w_here, keys, values = call(
        table_kernel,
        (
            shape(ROWS, TP * 8),
            shape(TP * 8, ROWS, dtype=F32),
            shape(TP * 8, ROWS, dtype=F32),
            pltpu.VMEM((TP, wlen, 128), BF16),
            cache,
            cache,
        ),
        [SMEM, HBM, HBM, HBM],
        [pltpu.SemaphoreType.DMA((3, OWN))],
    )(tp, in_hbm(w_own), in_hbm(keys_cache), in_hbm(values_cache))
    residual, sent = call(
        attend_kernel, (shape(OWN, D), shape(TP, 8, HALF)), [SMEM, SMEM] + [VMEM] * 8
    )(
        core,
        lengths,
        tokens,
        attn_in,
        in_vmem(w_here),
        in_vmem(w_sib),
        head_bias.reshape(1, HEADS),
        in_vmem(keys),
        in_vmem(values),
        gain_ffn.reshape(1, D),
    )
    group = a2a(sent, "x")
    group = group.reshape(TP * 8, HALF)
    rows = call(send_kernel, shape(ROWS, HALF), [VMEM] * 2)(pick, group)
    mix = call(mix_kernel, shape(TP * 8, 128, dtype=F32), [VMEM] * 2)(
        group, mix_gate.reshape(2, HALF)
    )
    combine = call(weigh_kernel, shape(2, TP * 8, ROWS), [VMEM] * 3)(
        mix, weight, mine
    )
    received = a2a(rows.reshape(CHIPS, MSG, HALF), ("z", "y"))
    outs = call(expert_kernel, shape(ROWS, HALF), [VMEM] * 4 + [HBM] + [VMEM] * 2, SIB_SCRATCH, 16)(
        received.reshape(ROWS, HALF),
        expert_gate[0],
        expert_up[0],
        expert_down[0],
        in_hbm(expert_sib),
        dense_own,
        dense_y,
    )
    returned = a2a(outs.reshape(CHIPS, MSG, HALF), ("z", "y"))
    partial = call(combine_kernel, shape(TP * 8, HALF), [VMEM] * 2)(
        combine, returned.reshape(ROWS, HALF)
    )
    parts = a2a(partial.reshape(TP, 8, HALF), "x")
    layer_out = call(finish_kernel, shape(OWN, D), [VMEM] * 2)(residual, parts)
    return (layer_out, new_keys, new_values)


def solution(mesh):
    grid = Mesh(mesh.devices.reshape(8, 8, 2, TP), ("z", "y", "c", "x"))
    ep = ("z", "y", "c")
    every = ("z", "y", "c", "x")
    return jax.shard_map(
        body,
        mesh=grid,
        in_specs=(
            P(every, None),
            P(),
            P(),
            P(None, "x"),
            P(),
            P(),
            P("x", None),
            P(),
            P(every, None, None),
            P(every, None, None),
            P(every),
            P(ep, None),
            P(ep, None),
            P(ep, None),
            P(),
            P(ep, None, "x"),
            P(ep, None, "x"),
            P(ep, "x", None),
            P(every, None),
            P(every, None),
        ),
        out_specs=(P(every, None), P(every, None), P(every, None)),
        check_vma=False,
    )
```

profile of v0, /device:TPU:8, one launch (start us, length us, event | category | flops | bytes accessed | tf_op | source)
XLA Modules:
  0.0 115.8 jit_solution(15909547021483913895)
XLA Ops:
  0.6 2.2 %shard_map.212 = (bf16[4,1032,128]{2,1,0:T(8,128)(2,1)}, bf16[96,1024]{1,0:T(8,128)(2,1)S(1)}) custom-call(s32[1]{0:T(128)} %bitcast.core, bf16[1024,128]{1,0:T(8,128)(2,1)} %wq.1, bf16[128,1024]{1,0:T(8,128)(2,1)} %wo.1, s32[2,4]{1,0:T(2,128)} %bitcast.26, f32[2,4]{1,0:T(2,128)} %bitcast.27, bf16[32,1024]{1,0:T(8,128)(2,1)} %gate.1, bf16[32,1024]{1,0:T(8,128)(2,1)} %up.1, ...), custom_call_target="tpu_custom_call" | custom-call | tf_op jit(solution)/shard_map/pallas_call | solution.py:399
  2.9 4.4 %all-to-all-start = ((bf16[4,1032,128]{2,1,0:T(8,128)(2,1)}), bf16[4,1032,128]{2,1,0:T(8,128)(2,1)}, u32[]{:S(2)}, u32[]{:S(2)}) async-start(bf16[4,1032,128]{2,1,0:T(8,128)(2,1)} %get-tuple-element.17), calls=%async_computation | async-start | bytes 2113536 | tf_op jit(solution)/shard_map/all_to_all | solution.py:367
  7.4 7.7 %collective-permute-start.1 = (bf16[96,1024]{1,0:T(8,128)(2,1)S(1)}, bf16[96,1024]{1,0:T(8,128)(2,1)S(1)}, u32[]{:S(2)}, u32[]{:S(2)}) collective-permute-start(bf16[96,1024]{1,0:T(8,128)(2,1)S(1)} %get-tuple-element.26.dense_own), channel_id=1, source_target_pairs={{0,8},{8,0},{16,24},{24,16},{32,40},{40,32},{48,56},{56,48},{1,9},... | collective-permute-start | bytes 589832 | tf_op jit(solution)/shard_map/ppermute | solution.py:371
  15.0 7.8 %all-to-all-done.own_hbm = bf16[4,1032,128]{2,1,0:T(8,128)(2,1)} async-done(((bf16[4,1032,128]{2,1,0:T(8,128)(2,1)}), bf16[4,1032,128]{2,1,0:T(8,128)(2,1)}, u32[]{:S(2)}, u32[]{:S(2)}) %all-to-all-start) | async-done | bytes 1056800 | tf_op jit(solution)/shard_map/all_to_all | solution.py:367
  22.8 1.9 %collective-permute-start = (bf16[4,1032,128]{2,1,0:T(8,128)(2,1)}, bf16[4,1032,128]{2,1,0:T(8,128)(2,1)S(1)}, u32[]{:S(2)}, u32[]{:S(2)}) collective-permute-start(bf16[4,1032,128]{2,1,0:T(8,128)(2,1)} %all-to-all-done.own_hbm), channel_id=1, source_target_pairs={{0,4},{4,0},{1,5},{5,1},{2,6},{6,2},{3,7},{7,3},{8,12},{12,8},{9,1... | collective-permute-start | bytes 3170312 | tf_op jit(solution)/shard_map/ppermute | solution.py:371
  24.8 1.4 %shard_map.218 = bf16[3840,256]{1,0:T(8,128)(2,1)} custom-call(bf16[1024,256]{1,0:T(8,128)(2,1)S(1)} %bitcast.14, bf16[1024,256]{1,0:T(8,128)(2,1)S(1)} %bitcast.16, bf16[256,1024]{1,0:T(8,128)(2,1)S(1)} %bitcast.18, bf16[96,1024]{1,0:T(8,128)(2,1)S(1)} %get-tuple-element.26.dense_own, bf16[96,1024]{1,0:T(8,128)(2,1)S(1)} %collective-permute-done.1.dense_y), custom_call_target="tpu_custom_call" | custom-call | tf_op jit(solution)/shard_map/pallas_call | solution.py:417
  26.2 2.4 %collective-permute-start.2 = (bf16[3840,256]{1,0:T(8,128)(2,1)}, bf16[3840,256]{1,0:T(8,128)(2,1)}, u32[]{:S(2)}, u32[]{:S(2)}) collective-permute-start(bf16[3840,256]{1,0:T(8,128)(2,1)} %shard_map.218), channel_id=1, source_target_pairs={{0,4},{4,0},{1,5},{5,1},{2,6},{6,2},{3,7},{7,3},{8,12},{12,8},{9,1... | collective-permute-start | bytes 5898248 | tf_op jit(solution)/shard_map/ppermute | solution.py:371
  28.6 0.7 reshape.43.gain
  29.3 0.7 reshape.46.gain
  30.0 0.8 shard_map.211
  30.8 1.9 %shard_map.213 = (bf16[512,32]{1,0:T(8,128)(2,1)S(1)}, f32[32,512]{1,0:T(8,128)S(1)}, f32[32,512]{1,0:T(8,128)S(1)}, bf16[4,1032,128]{2,1,0:T(8,128)(2,1)S(1)}, ...) custom-call(s32[1]{0:T(128)} %bitcast.1.tp, bf16[4,1032,128]{2,1,0:T(8,128)(2,1)} %all-to-all-done.own_hbm, ...), custom_call_target="tpu_custom_call" | custom-call | tf_op jit(solution)/shard_map/pallas_call | solution.py:425
  32.8 2.3 %shard_map.214 = (bf16[4,1024]{1,0:T(4,128)(2,1)S(1)}, bf16[4,8,512]{2,1,0:T(8,128)(2,1)S(1)}) custom-call(s32[1]{0:T(128)} %bitcast.core, s32[4]{0:T(128)S(1)} %copy-done.6, bf16[4,1024]{1,0:T(4,128)(2,1)S(1)} %copy-done.5, bf16[4,1024]{1,0:T(4,128)(2,1)S(1)} %get-tuple-element.16.attn_in, bf16[4,1032,128]{2,1,0:T(8,128)(2,1)S(1)} %get-tuple-element.18.w_own, ...), custom_call_target="tpu_custom_call" | custom-call | tf_op jit(solution)/shard_map/pallas_call | solution.py:438
  35.2 7.8 %all_to_all.25 = bf16[4,8,512]{2,1,0:T(8,128)(2,1)S(1)} all-to-all(bf16[4,8,512]{2,1,0:T(8,128)(2,1)S(1)} %get-tuple-element.22), channel_id=1, replica_groups=mesh['z'=8,'y'=8,'c'=2,'x'=4] {'x'}, dimensions={0} | all-to-all | bytes 65536 | tf_op jit(solution)/shard_map/all_to_all | solution.py:367
  43.0 1.1 shard_map.217
  44.1 16.6 %all-to-all-start.2 = ((bf16[64,8,512]{2,1,0:T(8,128)(2,1)}), bf16[64,8,512]{2,1,0:T(8,128)(2,1)S(1)}, u32[]{:S(2)}, u32[]{:S(2)}) async-start(bf16[64,8,512]{2,1,0:T(8,128)(2,1)} %bitcast.6), calls=%async_computation.2 | async-start | bytes 1048576 | tf_op jit(solution)/shard_map/all_to_all | solution.py:367
  60.7 18.5 %all-to-all-done.2 = bf16[64,8,512]{2,1,0:T(8,128)(2,1)S(1)} async-done(((bf16[64,8,512]{2,1,0:T(8,128)(2,1)}), bf16[64,8,512]{2,1,0:T(8,128)(2,1)S(1)}, u32[]{:S(2)}, u32[]{:S(2)}) %all-to-all-start.2) | async-done | bytes 524320 | tf_op jit(solution)/shard_map/all_to_all | solution.py:367
  79.2 4.5 %shard_map.219 = bf16[512,512]{1,0:T(8,128)(2,1)} custom-call(bf16[512,512]{1,0:T(8,128)(2,1)S(1)} %bitcast.20, bf16[1024,256]{1,0:T(8,128)(2,1)S(1)} %bitcast.15, bf16[1024,256]{1,0:T(8,128)(2,1)S(1)} %bitcast.17, bf16[256,1024]{1,0:T(8,128)(2,1)S(1)} %bitcast.19, bf16[3840,256]{1,0:T(8,128)(2,1)} %collective-permute-done.2.sib_hbm, ...), custom_call_target="tpu_custom_call" | custom-call | tf_op jit(solution)/shard_map/pallas_call | solution.py:462
  83.6 5.2 %all-to-all-start.3 = ((bf16[64,8,512]{2,1,0:T(8,128)(2,1)}), bf16[64,8,512]{2,1,0:T(8,128)(2,1)S(1)}, u32[]{:S(2)}, u32[]{:S(2)}) async-start(bf16[64,8,512]{2,1,0:T(8,128)(2,1)} %bitcast.11), calls=%async_computation.3 | async-start | bytes 1048576 | tf_op jit(solution)/shard_map/all_to_all | solution.py:367
  88.9 0.1 shard_map.215.mix
  89.0 0.1 shard_map.216.combine
  89.1 17.9 %all-to-all-done.3 = bf16[64,8,512]{2,1,0:T(8,128)(2,1)S(1)} async-done(((bf16[64,8,512]{2,1,0:T(8,128)(2,1)}), bf16[64,8,512]{2,1,0:T(8,128)(2,1)S(1)}, u32[]{:S(2)}, u32[]{:S(2)}) %all-to-all-start.3) | async-done | bytes 524320 | tf_op jit(solution)/shard_map/all_to_all | solution.py:367
  107.0 0.3 shard_map.220
  107.2 8.0 %all_to_all.26.parts = bf16[4,8,512]{2,1,0:T(8,128)(2,1)S(1)} all-to-all(bf16[4,8,512]{2,1,0:T(8,128)(2,1)S(1)} %bitcast.24), channel_id=1, replica_groups=mesh['z'=8,'y'=8,'c'=2,'x'=4] {'x'}, dimensions={0} | all-to-all | bytes 65536 | tf_op jit(solution)/shard_map/all_to_all | solution.py:367
  115.2 0.6 shard_map.221
  (22 shorter events, 0.1 us)
Async XLA Ops:
  2.9 21.9 %copy-start = (bf16[1,1024,256]{2,1,0:T(8,128)(2,1)S(1)}, bf16[1,1024,256]{2,1,0:T(8,128)(2,1)}, u32[]{:S(2)}) copy-start(bf16[1,1024,256]{2,1,0:T(8,128)(2,1)} %param.35) | copy-start | bytes 1572868
  2.9 21.9 %copy-start.1 = (bf16[1,1024,256]{2,1,0:T(8,128)(2,1)S(1)}, bf16[1,1024,256]{2,1,0:T(8,128)(2,1)}, u32[]{:S(2)}) copy-start(bf16[1,1024,256]{2,1,0:T(8,128)(2,1)} %param.36) | copy-start | bytes 1572868
  2.9 21.9 %copy-start.2 = (bf16[1,256,1024]{2,1,0:T(8,128)(2,1)S(1)}, bf16[1,256,1024]{2,1,0:T(8,128)(2,1)}, u32[]{:S(2)}) copy-start(bf16[1,256,1024]{2,1,0:T(8,128)(2,1)} %param.37) | copy-start | bytes 1572868
  2.9 19.9 %all-to-all-start = ((bf16[4,1032,128]{2,1,0:T(8,128)(2,1)}), bf16[4,1032,128]{2,1,0:T(8,128)(2,1)}, u32[]{:S(2)}, u32[]{:S(2)}) async-start(bf16[4,1032,128]{2,1,0:T(8,128)(2,1)} %get-tuple-element.17), calls=%async_computation | async-start | bytes 2113536 | tf_op jit(solution)/shard_map/all_to_all | solution.py:367
  7.4 17.4 %collective-permute-start.1 = (bf16[96,1024]{1,0:T(8,128)(2,1)S(1)}, bf16[96,1024]{1,0:T(8,128)(2,1)S(1)}, u32[]{:S(2)}, u32[]{:S(2)}) collective-permute-start(bf16[96,1024]{1,0:T(8,128)(2,1)S(1)} %get-tuple-element.26.dense_own), channel_id=1, source_target_pairs={{0,8},{8,0},{16,24},{24,16},{32,40},{40,32},{48,56},{56,48},{1,9},... | collective-permute-start | bytes 589832 | tf_op jit(solution)/shard_map/ppermute | solution.py:371
  22.8 10.0 %collective-permute-start = (bf16[4,1032,128]{2,1,0:T(8,128)(2,1)}, bf16[4,1032,128]{2,1,0:T(8,128)(2,1)S(1)}, u32[]{:S(2)}, u32[]{:S(2)}) collective-permute-start(bf16[4,1032,128]{2,1,0:T(8,128)(2,1)} %all-to-all-done.own_hbm), channel_id=1, source_target_pairs={{0,4},{4,0},{1,5},{5,1},{2,6},{6,2},{3,7},{7,3},{8,12},{12,8},{9,1... | collective-permute-start | bytes 3170312 | tf_op jit(solution)/shard_map/ppermute | solution.py:371
  24.8 5.2 %copy-start.3 = (bf16[1024,128]{1,0:T(8,128)(2,1)S(1)}, bf16[1024,128]{1,0:T(8,128)(2,1)}, u32[]{:S(2)}) copy-start(bf16[1024,128]{1,0:T(8,128)(2,1)} %wk.1) | copy-start | bytes 786436
  24.8 5.2 %copy-start.4 = (bf16[1024,128]{1,0:T(8,128)(2,1)S(1)}, bf16[1024,128]{1,0:T(8,128)(2,1)}, u32[]{:S(2)}) copy-start(bf16[1024,128]{1,0:T(8,128)(2,1)} %wv.1) | copy-start | bytes 786436
  24.8 5.2 %copy-start.5 = (bf16[4,1024]{1,0:T(4,128)(2,1)S(1)}, bf16[4,1024]{1,0:T(4,128)(2,1)}, u32[]{:S(2)}) copy-start(bf16[4,1024]{1,0:T(4,128)(2,1)} %tokens.3) | copy-start | bytes 24580
  26.2 34.4 %collective-permute-start.2 = (bf16[3840,256]{1,0:T(8,128)(2,1)}, bf16[3840,256]{1,0:T(8,128)(2,1)}, u32[]{:S(2)}, u32[]{:S(2)}) collective-permute-start(bf16[3840,256]{1,0:T(8,128)(2,1)} %shard_map.218), channel_id=1, source_target_pairs={{0,4},{4,0},{1,5},{5,1},{2,6},{6,2},{3,7},{7,3},{8,12},{12,8},{9,1... | collective-permute-start | bytes 5898248 | tf_op jit(solution)/shard_map/ppermute | solution.py:371
  30.8 2.0 %copy-start.6 = (s32[4]{0:T(128)S(1)}, s32[4]{0:T(128)}, u32[]{:S(2)}) copy-start(s32[4]{0:T(128)} %lengths.1) | copy-start | bytes 52
  30.8 2.0 %copy-start.7 = (f32[8]{0:T(128)S(1)}, f32[8]{0:T(128)}, u32[]{:S(2)}) copy-start(f32[8]{0:T(128)} %param.27) | copy-start | bytes 100
  44.1 35.1 %all-to-all-start.2 = ((bf16[64,8,512]{2,1,0:T(8,128)(2,1)}), bf16[64,8,512]{2,1,0:T(8,128)(2,1)S(1)}, u32[]{:S(2)}, u32[]{:S(2)}) async-start(bf16[64,8,512]{2,1,0:T(8,128)(2,1)} %bitcast.6), calls=%async_computation.2 | async-start | bytes 1048576 | tf_op jit(solution)/shard_map/all_to_all | solution.py:367
  79.2 9.7 %copy-start.8 = (bf16[1024]{0:T(1024)(128)(2,1)S(1)}, bf16[1024]{0:T(1024)(128)(2,1)}, u32[]{:S(2)}) copy-start(bf16[1024]{0:T(1024)(128)(2,1)} %param.34) | copy-start | bytes 6148
  83.6 23.4 %all-to-all-start.3 = ((bf16[64,8,512]{2,1,0:T(8,128)(2,1)}), bf16[64,8,512]{2,1,0:T(8,128)(2,1)S(1)}, u32[]{:S(2)}, u32[]{:S(2)}) async-start(bf16[64,8,512]{2,1,0:T(8,128)(2,1)} %bitcast.11), calls=%async_computation.3 | async-start | bytes 1048576 | tf_op jit(solution)/shard_map/all_to_all | solution.py:367
where the time goes:
time: 116 us
  waiting for transfers between devices  44.2 us (38%)
  starting transfers between devices  38.2 us (33%)
  blocking collectives  15.8 us (14%)
  Pallas kernels  15.4 us (13%)
  local copies, waits for them, and re-layouts  1.43 us (1%)
    all_to_all x3, waiting for transfers between devices, a2a(): return lax.all_to_all(array, axis, split_axis=0, concat_axis=0, tiled=True)  44.2 us
    all_to_all x3, starting transfers between devices, a2a(): return lax.all_to_all(array, axis, split_axis=0, concat_axis=0, tiled=True)  26.3 us
    all_to_all x2, blocking collectives, a2a(): return lax.all_to_all(array, axis, split_axis=0, concat_axis=0, tiled=True)  15.8 us
    ppermute x3, starting transfers between devices, swap(): lax.ppermute(array, axis, [(i, i ^ 1) for i in range(lax.axis_size(axis))])  12 us
    pallas_call x1, Pallas kernels, body(): call(expert_kernel, shape(ROWS, HALF), [VMEM] * 4 + [HBM] + [VMEM] * 2, S...  4.45 us
    pallas_call x1, Pallas kernels, body(): call(attend_kernel, (shape(OWN, D), shape(TP, 8, HALF)), [SMEM, SMEM] + [...  2.34 us
  transfers between devices with their start and end apart: 6, of which 3 were waited for; matrix products, arithmetic and copies ran while one was open for 1% of the time, Pallas kernels for 7%

commit v1 on v0

--- a/solution.py
+++ b/solution.py
@@ -29,10 +29,7 @@
 HBM = pl.BlockSpec(memory_space=pltpu.HBM)
 EXPERT_ROWS = 3 * D
 DENSE_ROWS = 96
-SIB_SCRATCH = [
-    pltpu.VMEM((EXPERT_ROWS + 8 * DENSE_ROWS, 256), jnp.bfloat16),
-    pltpu.SemaphoreType.DMA((7,)),
-]
+PACK = EXPERT_ROWS + 4 * DENSE_ROWS
 
 
 def dot(a, b):
@@ -47,8 +44,8 @@
     return lax.broadcasted_iota(jnp.int32, shape, dim)
 
 
-def call(kernel, out_shape, specs, scratch=(), limit=4):
-    outs = jax.tree.map(lambda _: VMEM, out_shape)
+def call(kernel, out_shape, specs, scratch=(), limit=4, outs=VMEM):
+    outs = jax.tree.map(lambda _: outs, out_shape)
     return pl.pallas_call(
         kernel,
         out_shape=out_shape,
@@ -65,32 +62,24 @@
     return (wide * scale) * gains.astype(F32)
 
 
-def pack_kernel(core, wq, wo, routes_hbm, weights_hbm, gate, up, down, out, dense, routes, weights, sems):
+def pack_kernel(
+    core, wq, wo, routes_hbm, weights_hbm, gate, up, down, out, dense, routes, weights, half, rows, sems
+):
     start = core[0] * HALF
     facts = [
-        pltpu.make_async_copy(routes_hbm, routes, sems.at[8]),
-        pltpu.make_async_copy(weights_hbm, weights, sems.at[9]),
+        pltpu.make_async_copy(routes_hbm, routes, sems.at[0]),
+        pltpu.make_async_copy(weights_hbm, weights, sems.at[1]),
     ]
-    for c in facts:
-        c.start()
-    copies = [
-        pltpu.make_async_copy(
-            wq.at[pl.ds(pl.multiple_of(start, HALF), HALF), :], out.at[0, 0:HALF, :], sems.at[0]
-        )
+    reads = [(wq.at[pl.ds(pl.multiple_of(start, HALF), HALF), :], half.at[0:HALF, :])]
+    for j in range(4):
+        block = wo.at[:, pl.ds(pl.multiple_of(start + j * 128, 128), 128)]
+        reads.append((block, half.at[HALF + 128 * j : HALF + 128 * (j + 1), :]))
+    reads = [pltpu.make_async_copy(a, b, sems.at[2 + k]) for k, (a, b) in enumerate(reads)]
+    shared = [
+        pltpu.make_async_copy(ref, rows.at[32 * k : 32 * (k + 1), :], sems.at[7 + k])
+        for k, ref in enumerate((gate, up, down))
     ]
-    for j in range(4):
-        copies.append(
-            pltpu.make_async_copy(
-                wo.at[:, pl.ds(pl.multiple_of(start + j * 128, 128), 128)],
-                out.at[0, HALF + 128 * j : HALF + 128 * (j + 1), :],
-                sems.at[1 + j],
-            )
-        )
-    for k, ref in enumerate((gate, up, down)):
-        copies.append(
-            pltpu.make_async_copy(ref, dense.at[32 * k : 32 * (k + 1), :], sems.at[5 + k])
-        )
-    for c in copies:
+    for c in facts + reads + shared:
         c.start()
     for c in facts:
         c.wait()
@@ -106,31 +95,75 @@
     info = jnp.zeros((OWN, 128), F32)
     for place, row in enumerate((ids[0:1], ids[1:2], high[0:1], low[0:1], high[1:2], low[1:2])):
         info = jnp.where(lane == place, column(row), info)
-    info = jnp.concatenate([info, info], axis=0).astype(BF16)
-    for d in range(TP):
-        out[d, 2 * HALF : 2 * HALF + 8, :] = info
+    half[2 * HALF : 2 * HALF + 8, :] = jnp.concatenate([info, info], axis=0).astype(BF16)
+    for c in reads:
+        c.wait()
+    sends = [pltpu.make_async_copy(half, out.at[d], sems.at[10 + d]) for d in range(TP)]
+    for c in sends:
+        c.start()
+    for c in shared:
+        c.wait()
+    last = pltpu.make_async_copy(rows, dense, sems.at[14])
+    last.start()
+    for c in sends:
+        c.wait()
+    last.wait()
+
+
+def norm_kernel(tokens, gain, attn_in):
+    attn_in[...] = rms(tokens[...], gain[...]).astype(BF16)
+
+
+def kv_kernel(attn_in, wk, wv, new_k, new_v):
+    a = attn_in[...]
+    new_k[...] = dot(a, wk[...]).astype(BF16)
+    new_v[...] = dot(a, wv[...]).astype(BF16)
+
+
+def expert_pack_kernel(gate, up, down, dense, out, here, sems):
+    reads = [
+        (ref.at[h * HALF : (h + 1) * HALF, :], D * k + HALF * h, HALF)
+        for k, ref in enumerate((gate, up))
+        for h in range(2)
+    ]
+    base = 2 * D
+    for ref in (down, dense):
+        n = ref.shape[0]
+        for j in range(4):
+            reads.append((ref.at[:, 256 * j : 256 * (j + 1)], base, n))
+            base = base + n
+    ins, outs = [], []
+    for k, (src, first, n) in enumerate(reads):
+        place = here.at[first : first + n, :]
+        ins.append(pltpu.make_async_copy(src, place, sems.at[0, k]))
+        outs.append(pltpu.make_async_copy(place, out.at[first : first + n, :], sems.at[1, k]))
+    for c in ins:
+        c.start()
+    for a, b in zip(ins, outs):
+        a.wait()
+        b.start()
+    for c in outs:
+        c.wait()
+
+
+def fetch_kernel(*refs):
+    n = (len(refs) - 1) // 2
+    sems = refs[-1]
+    copies = []
+    for k in range(n):
+        rows = refs[k].shape[0]
+        step = rows // 4
+        for q in range(4):
+            part = slice(q * step, (q + 1) * step)
+            copies.append(
+                pltpu.make_async_copy(
+                    refs[k].at[part, :], refs[n + k].at[part, :], sems.at[k, q]
+                )
+            )
+    for c in copies:
+        c.start()
     for c in copies:
         c.wait()
-    for d in range(1, TP):
-        out[d, 0 : 2 * HALF, :] = out[0, 0 : 2 * HALF, :]
-
-
-def norm_kernel(tokens, gain, wk, wv, attn_in, new_k, new_v):
-    a = rms(tokens[...], gain[...]).astype(BF16)
-    attn_in[...] = a
-    new_k[...] = dot(a, wk[...]).astype(BF16)
-    new_v[...] = dot(a, wv[...]).astype(BF16)
-
-
-def expert_pack_kernel(gate, up, down, dense_own, dense_y, out):
-    out[0:D, :] = gate[...]
-    out[D : 2 * D, :] = up[...]
-    base = 2 * D
-    for ref in (down, dense_own, dense_y):
-        n = ref.shape[0]
-        for j in range(4):
-            out[base : base + n, :] = ref[:, 256 * j : 256 * (j + 1)]
-            base = base + n
 
 
 def attend_kernel(
@@ -262,8 +295,12 @@
             c.wait()
 
 
-def send_kernel(pick, group, sent):
-    sent[...] = dot(pick[...], group[...]).astype(BF16)
+def send_kernel(pick, group, out, here, sems):
+    for b in range(ROWS // 256):
+        part = dot(pick[256 * b : 256 * (b + 1), :], group[...])
+        send_rows(part, here, out, 256 * b, sems.at[b])
+    for b in range(ROWS // 256):
+        send_wait(here, out, 256 * b, sems.at[b])
 
 
 def mix_kernel(group, mix_gate, mix):
@@ -284,57 +321,81 @@
     combine[1] = (total - high.astype(F32)).astype(BF16)
 
 
-def expert_kernel(x, gate, up, down, sib_hbm, dense_own, dense_y, out, sib, sems):
-    edges = [0, D // 2, D, 3 * D // 2, 2 * D, 5 * D // 2, EXPERT_ROWS, EXPERT_ROWS + 8 * DENSE_ROWS]
+def rows_copy(here, out, first, sem):
+    part = slice(first, first + 256)
+    return pltpu.make_async_copy(here.at[part, :], out.at[part, :], sem)
+
+
+def send_rows(values, here, out, first, sem):
+    here[first : first + 256, :] = values.astype(BF16)
+    rows_copy(here, out, first, sem).start()
+
+
+def send_wait(here, out, first, sem):
+    rows_copy(here, out, first, sem).wait()
+
+
+def expert_kernel(x, own_hbm, sib, dense_y, dense_yc, out, own, here, sems):
+    step = PACK // 8
     copies = [
-        pltpu.make_async_copy(sib_hbm.at[lo:hi, :], sib.at[lo:hi, :], sems.at[k])
-        for k, (lo, hi) in enumerate(zip(edges[:-1], edges[1:]))
+        pltpu.make_async_copy(
+            own_hbm.at[k * step : (k + 1) * step, :], own.at[k * step : (k + 1) * step, :], sems.at[k]
+        )
+        for k in range(8)
     ]
     for c in copies:
         c.start()
-    rows = CHIPS * 4
-    i, k = iota((rows, ROWS), 0), iota((rows, ROWS), 1)
-    at = (i // 4) * MSG + i % 4
-    halves = [(k == at + 4 * h).astype(F32).astype(BF16) for h in range(2)]
-    got = x[...]
-    xs = jnp.concatenate([dot(p, got) for p in halves], axis=1).astype(BF16)
-    is_slot = iota((rows, 1), 0) % 4 < 2
-
-    def hidden(g, u, keep):
-        return jnp.where(keep, g / (1.0 + jnp.exp(-g)) * u, 0.0).astype(BF16)
-
-    h_own = hidden(dot(xs, gate[...]), dot(xs, up[...]), is_slot)
-    total = dot(h_own, down[...])
-    for c in copies:
-        c.wait()
-    h_sib = hidden(dot(xs, sib[0:D, :]), dot(xs, sib[D : 2 * D, :]), is_slot)
+
+    def place(dim):
+        k = iota((256, 256), dim)
+        i = k % 64
+        return (i // 2) * MSG + i % 2 + 2 * (k // 64 % 2) + 4 * (k // 128)
+
+    order = (iota((256, 256), 1) == place(0)).astype(F32).astype(BF16)
+    back = (iota((256, 256), 0) == place(1)).astype(F32).astype(BF16)
+    blocks = ROWS // 256
+    xs, xd = [], []
+    for b in range(blocks):
+        y = dot(order, x[256 * b : 256 * (b + 1), :]).astype(BF16)
+        xs.append(jnp.concatenate([y[0:64], y[128:192]], axis=1))
+        xd.append(jnp.concatenate([y[64:128], y[192:256]], axis=1))
+    xs, xd = jnp.concatenate(xs, axis=0), jnp.concatenate(xd, axis=0)
+
+    def hidden(g, u):
+        return (g / (1.0 + jnp.exp(-g)) * u).astype(BF16)
+
+    total = None
+    for w in (sib, own):
+        if w is own:
+            for c in copies:
+                c.wait()
+        h = hidden(dot(xs, w[0:D, :]), dot(xs, w[D : 2 * D, :]))
+        part = jnp.concatenate(
+            [dot(h, w[2 * D + 256 * j : 2 * D + 256 * (j + 1), :]) for j in range(4)], axis=1
+        )
+        total = part if total is None else total + part
 
     def stack(base):
-        parts = [ref[base : base + 32, :] for ref in (dense_own, dense_y)]
-        for k in range(2):
-            first = EXPERT_ROWS + 4 * DENSE_ROWS * k + base
+        parts = [ref[base : base + 32, :] for ref in (dense_y, dense_yc)]
+        for w in (own, sib):
+            first = EXPERT_ROWS + base
             parts.append(
                 jnp.concatenate(
-                    [sib[first + DENSE_ROWS * j : first + DENSE_ROWS * j + 32, :] for j in range(4)],
+                    [w[first + DENSE_ROWS * j : first + DENSE_ROWS * j + 32, :] for j in range(4)],
                     axis=1,
                 )
             )
         return jnp.concatenate(parts, axis=0)
 
-    h_dense = hidden(dot_t(xs, stack(0)), dot_t(xs, stack(32)), jnp.logical_not(is_slot))
-    total = total + dot(h_dense, stack(64))
-    total = total + jnp.concatenate(
-        [dot(h_sib, sib[2 * D + 256 * j : 2 * D + 256 * (j + 1), :]) for j in range(4)], axis=1
-    )
+    h_dense = hidden(dot_t(xd, stack(0)), dot_t(xd, stack(32)))
+    dense = dot(h_dense, stack(64)).astype(BF16)
     total = total.astype(BF16)
-    i, k = iota((ROWS, rows), 1), iota((ROWS, rows), 0)
-    at = (i // 4) * MSG + i % 4
-    res = None
-    for h in range(2):
-        p = (k == at + 4 * h).astype(F32).astype(BF16)
-        part = dot(p, total[:, HALF * h : HALF * (h + 1)])
-        res = part if res is None else res + part
-    out[...] = res.astype(BF16)
+    for b in range(blocks):
+        part = jnp.concatenate([total[64 * b : 64 * (b + 1)], dense[64 * b : 64 * (b + 1)]], axis=0)
+        part = jnp.concatenate([part[:, :HALF], part[:, HALF:]], axis=0)
+        send_rows(dot(back, part), here, out, 256 * b, sems.at[8 + b])
+    for b in range(blocks):
+        send_wait(here, out, 256 * b, sems.at[8 + b])
 
 
 def combine_kernel(combine, returned, out):
@@ -398,9 +459,16 @@
     wlen = 2 * HALF + 8
     packed, dense_own = call(
         pack_kernel,
-        (shape(TP, wlen, 128), shape(DENSE_ROWS, D)),
+        (pltpu.HBM((TP, wlen, 128), BF16), pltpu.HBM((DENSE_ROWS, D), BF16)),
         [SMEM] + [HBM] * 7,
-        [pltpu.VMEM((2, OWN), jnp.int32), pltpu.VMEM((2, OWN), F32), pltpu.SemaphoreType.DMA((10,))],
+        [
+            pltpu.VMEM((2, OWN), jnp.int32),
+            pltpu.VMEM((2, OWN), F32),
+            pltpu.VMEM((wlen, 128), BF16),
+            pltpu.VMEM((DENSE_ROWS, D), BF16),
+            pltpu.SemaphoreType.DMA((15,)),
+        ],
+        outs=HBM,
     )(
         core,
         in_hbm(w_query),
@@ -415,12 +483,23 @@
     w_sib = swap(w_own, "c")
     dense_y = swap(dense_own, "y")
     expert_own = call(
-        expert_pack_kernel, shape(EXPERT_ROWS + 8 * DENSE_ROWS, 256), [VMEM] * 5, limit=8
-    )(expert_gate[0], expert_up[0], expert_down[0], dense_own, dense_y)
+        expert_pack_kernel,
+        pltpu.HBM((PACK, 256), BF16),
+        [HBM] * 4,
+        [pltpu.VMEM((PACK, 256), BF16), pltpu.SemaphoreType.DMA((2, 12))],
+        outs=HBM,
+    )(
+        in_hbm(expert_gate[0]),
+        in_hbm(expert_up[0]),
+        in_hbm(expert_down[0]),
+        in_hbm(dense_own),
+    )
     expert_sib = swap(expert_own, "c")
-    attn_in, new_keys, new_values = call(
-        norm_kernel, (shape(OWN, D), shape(OWN, 128), shape(OWN, 128)), [VMEM] * 4
-    )(tokens, gain_attn.reshape(1, D), w_key, w_value)
+    dense_yc = swap(dense_y, "c")
+    attn_in = call(norm_kernel, shape(OWN, D), [VMEM] * 2)(tokens, gain_attn.reshape(1, D))
+    new_keys, new_values = call(
+        kv_kernel, (shape(OWN, 128), shape(OWN, 128)), [VMEM] * 3
+    )(attn_in, w_key, w_value)
     cache = pltpu.VMEM((OWN, CACHE, 128), BF16)
     pick, weight, mine, w_here, keys, values = call(
         table_kernel,
@@ -451,7 +530,13 @@
     )
     group = a2a(sent, "x")
     group = group.reshape(TP * 8, HALF)
-    rows = call(send_kernel, shape(ROWS, HALF), [VMEM] * 2)(pick, group)
+    rows = call(
+        send_kernel,
+        pltpu.HBM((ROWS, HALF), BF16),
+        [VMEM] * 2,
+        [pltpu.VMEM((ROWS, HALF), BF16), pltpu.SemaphoreType.DMA((2,))],
+        outs=HBM,
+    )(pick, group)
     mix = call(mix_kernel, shape(TP * 8, 128, dtype=F32), [VMEM] * 2)(
         group, mix_gate.reshape(2, HALF)
     )
@@ -459,15 +544,26 @@
         mix, weight, mine
     )
     received = a2a(rows.reshape(CHIPS, MSG, HALF), ("z", "y"))
-    outs = call(expert_kernel, shape(ROWS, HALF), [VMEM] * 4 + [HBM] + [VMEM] * 2, SIB_SCRATCH, 16)(
-        received.reshape(ROWS, HALF),
-        expert_gate[0],
-        expert_up[0],
-        expert_down[0],
-        in_hbm(expert_sib),
-        dense_own,
-        dense_y,
-    )
+    sources = (expert_sib, dense_y, dense_yc)
+    fetched = call(
+        fetch_kernel,
+        tuple(pltpu.VMEM(a.shape, BF16) for a in sources),
+        [HBM] * 3,
+        [pltpu.SemaphoreType.DMA((3, 4))],
+        8,
+    )(*(in_hbm(a) for a in sources))
+    outs = call(
+        expert_kernel,
+        pltpu.HBM((ROWS, HALF), BF16),
+        [VMEM, HBM] + [VMEM] * 3,
+        [
+            pltpu.VMEM((PACK, 256), BF16),
+            pltpu.VMEM((ROWS, HALF), BF16),
+            pltpu.SemaphoreType.DMA((10,)),
+        ],
+        16,
+        HBM,
+    )(received.reshape(ROWS, HALF), in_hbm(expert_own), *(in_vmem(a) for a in fetched))
     returned = a2a(outs.reshape(CHIPS, MSG, HALF), ("z", "y"))
     partial = call(combine_kernel, shape(TP * 8, HALF), [VMEM] * 2)(
         combine, returned.reshape(ROWS, HALF)

time: 116 us -> 126 us (1.086)
  blocking collectives: 15.8 us -> 27.4 us
  waiting for transfers between devices: 44.2 us -> 38 us
  starting transfers between devices: 38.2 us -> 41.2 us
  Pallas kernels: 15.4 us -> 17.4 us
    all_to_all x3, waiting for transfers between devices: 44.2 us -> 23.9 us  [a2a(): return lax.all_to_all(array, axis, split_axis=0, concat_axis=0, tiled=True)]
    ppermute x3 -> x4, waiting for transfers between devices: 0.01 us -> 14.1 us  [swap(): lax.ppermute(array, axis, [(i, i ^ 1) for i in range(lax.axis_size(axis))])]
    all_to_all x2, blocking collectives: 15.8 us -> 27.4 us  [a2a(): return lax.all_to_all(array, axis, split_axis=0, concat_axis=0, tiled=True)]
    all_to_all x3, starting transfers between devices: 26.3 us -> 32.7 us  [a2a(): return lax.all_to_all(array, axis, split_axis=0, concat_axis=0, tiled=True)]
    ppermute x3 -> x4, starting transfers between devices: 12 us -> 8.59 us  [swap(): lax.ppermute(array, axis, [(i, i ^ 1) for i in range(lax.axis_size(axis))])]
    pallas_call x5 -> x7, Pallas kernels: 9.99 us -> 11.4 us  [the longest x1 3.47 us: body(): call(expert_kernel, pltpu.HBM((ROWS, HALF), BF16), [VMEM, HBM] + [VMEM] *...]
  transfers between devices with their start and end apart: 6 -> 7, of which waited for: 3 -> 4; matrix products, arithmetic and copies ran while one was open for 1% -> 0% of each run, Pallas kernels for 7% -> 8%
where the time goes in v1:
time: 126 us
  starting transfers between devices  41.2 us (33%)
  waiting for transfers between devices  38 us (30%)
  blocking collectives  27.4 us (22%)
  Pallas kernels  17.4 us (14%)
    all_to_all x3, starting transfers between devices, a2a(): return lax.all_to_all(array, axis, split_axis=0, concat_axis=0, tiled=True)  32.7 us
    all_to_all x2, blocking collectives, a2a(): return lax.all_to_all(array, axis, split_axis=0, concat_axis=0, tiled=True)  27.4 us
    all_to_all x3, waiting for transfers between devices, a2a(): return lax.all_to_all(array, axis, split_axis=0, concat_axis=0, tiled=True)  23.9 us
    ppermute x4, waiting for transfers between devices, swap(): lax.ppermute(array, axis, [(i, i ^ 1) for i in range(lax.axis_size(axis))])  14.1 us
    ppermute x4, starting transfers between devices, swap(): lax.ppermute(array, axis, [(i, i ^ 1) for i in range(lax.axis_size(axis))])  8.59 us
    pallas_call x1, Pallas kernels, body(): call(expert_kernel, pltpu.HBM((ROWS, HALF), BF16), [VMEM, HBM] + [VMEM] *...  3.47 us
  transfers between devices with their start and end apart: 7, of which 4 were waited for; matrix products, arithmetic and copies ran while one was open for 0% of the time, Pallas kernels for 8%

profile of v1, /device:TPU:8, one launch (start us, length us, event | category | flops | bytes accessed | tf_op | source)
XLA Modules:
  0.0 125.8 jit_solution(14961815949933288391)
XLA Ops:
  0.6 2.1 %shard_map.212 = (bf16[4,1032,128]{2,1,0:T(8,128)(2,1)}, bf16[96,1024]{1,0:T(8,128)(2,1)}) custom-call(s32[1]{0:T(128)} %bitcast.core, bf16[1024,128]{1,0:T(8,128)(2,1)} %wq.1, bf16[128,1024]{1,0:T(8,128)(2,1)} %wo.1, s32[2,4]{1,0:T(2,128)} %bitcast.24, f32[2,4]{1,0:T(2,128)} %bitcast.25, bf16[32,1024]{1,0:T(8,128)(2,1)} %gate.1, bf16[32,1024]{1,0:T(8,128)(2,1)} %up.1, ...), custom_call_target="tpu_custom_call" | custom-call | tf_op jit(solution)/shard_map/pallas_call | solution.py:460
  2.8 19.5 %all_to_all.25.own_hbm = bf16[4,1032,128]{2,1,0:T(8,128)(2,1)S(1)} all-to-all(bf16[4,1032,128]{2,1,0:T(8,128)(2,1)} %get-tuple-element.18), channel_id=1, replica_groups=mesh['z'=8,'y'=8,'c'=2,'x'=4] {'x'}, dimensions={0} | all-to-all | bytes 2113536 | tf_op jit(solution)/shard_map/all_to_all | solution.py:428
  22.3 1.9 %collective-permute-start = (bf16[4,1032,128]{2,1,0:T(8,128)(2,1)S(1)}, bf16[4,1032,128]{2,1,0:T(8,128)(2,1)S(1)}, u32[]{:S(2)}, u32[]{:S(2)}) collective-permute-start(bf16[4,1032,128]{2,1,0:T(8,128)(2,1)S(1)} %all_to_all.25.own_hbm), channel_id=1, source_target_pairs={{0,4},{4,0},{1,5},{5,1},{2,6},{6,2},{3,7},{7,3},{8,12},{12,8},{9,1... | collective-permute-start | bytes 3170312 | tf_op jit(solution)/shard_map/ppermute | solution.py:432
  24.2 2.4 %shard_map.218.own_hbm = bf16[3456,256]{1,0:T(8,128)(2,1)} custom-call(bf16[1024,256]{1,0:T(8,128)(2,1)} %bitcast.21, bf16[1024,256]{1,0:T(8,128)(2,1)} %bitcast.22, bf16[256,1024]{1,0:T(8,128)(2,1)} %bitcast.23, bf16[96,1024]{1,0:T(8,128)(2,1)} %get-tuple-element.27.dense), custom_call_target="tpu_custom_call" | custom-call | tf_op jit(solution)/shard_map/pallas_call | solution.py:485
  26.7 2.4 %collective-permute-start.1 = (bf16[3456,256]{1,0:T(8,128)(2,1)}, bf16[3456,256]{1,0:T(8,128)(2,1)}, u32[]{:S(2)}, u32[]{:S(2)}) collective-permute-start(bf16[3456,256]{1,0:T(8,128)(2,1)} %shard_map.218.own_hbm), channel_id=1, source_target_pairs={{0,4},{4,0},{1,5},{5,1},{2,6},{6,2},{3,7},{7,3},{8,12},{12,8},{9,1... | collective-permute-start | bytes 5308424 | tf_op jit(solution)/shard_map/ppermute | solution.py:432
  29.3 2.0 %shard_map.213 = (bf16[512,32]{1,0:T(8,128)(2,1)S(1)}, f32[32,512]{1,0:T(8,128)S(1)}, f32[32,512]{1,0:T(8,128)S(1)}, bf16[4,1032,128]{2,1,0:T(8,128)(2,1)S(1)}, ...) custom-call(s32[1]{0:T(128)} %bitcast.1.tp, bf16[4,1032,128]{2,1,0:T(8,128)(2,1)} %copy-done.5, ...), custom_call_target="tpu_custom_call" | custom-call | tf_op jit(solution)/shard_map/pallas_call | solution.py:504
  31.2 2.3 %shard_map.214 = (bf16[4,1024]{1,0:T(4,128)(2,1)S(1)}, bf16[4,8,512]{2,1,0:T(8,128)(2,1)S(1)}) custom-call(s32[1]{0:T(128)} %bitcast.core, s32[4]{0:T(128)S(1)} %copy-done.3, bf16[4,1024]{1,0:T(4,128)(2,1)S(1)} %copy-done.2, bf16[4,1024]{1,0:T(4,128)(2,1)S(1)} %shard_map.211.attn_in, bf16[4,1032,128]{2,1,0:T(8,128)(2,1)S(1)} %get-tuple-element.19.w_own, ...), custom_call_target="tpu_custom_call" | custom-call | tf_op jit(solution)/shard_map/pallas_call | solution.py:517
  33.6 7.9 %all_to_all.26 = bf16[4,8,512]{2,1,0:T(8,128)(2,1)S(1)} all-to-all(bf16[4,8,512]{2,1,0:T(8,128)(2,1)S(1)} %get-tuple-element.23), channel_id=1, replica_groups=mesh['z'=8,'y'=8,'c'=2,'x'=4] {'x'}, dimensions={0} | all-to-all | bytes 65536 | tf_op jit(solution)/shard_map/all_to_all | solution.py:428
  41.5 1.0 shard_map.217
  42.5 16.6 %all-to-all-start.2 = ((bf16[64,8,512]{2,1,0:T(8,128)(2,1)}), bf16[64,8,512]{2,1,0:T(8,128)(2,1)S(1)}, u32[]{:S(2)}, u32[]{:S(2)}) async-start(bf16[64,8,512]{2,1,0:T(8,128)(2,1)} %bitcast.20), calls=%async_computation.2 | async-start | bytes 1048576 | tf_op jit(solution)/shard_map/all_to_all | solution.py:428
  59.2 2.4 %collective-permute-start.2 = (bf16[96,1024]{1,0:T(8,128)(2,1)S(1)}, bf16[96,1024]{1,0:T(8,128)(2,1)S(1)}, u32[]{:S(2)}, u32[]{:S(2)}) collective-permute-start(bf16[96,1024]{1,0:T(8,128)(2,1)S(1)} %copy-done.6), channel_id=1, source_target_pairs={{0,8},{8,0},{16,24},{24,16},{32,40},{40,32},{48,56},{56,48},{1,9},... | collective-permute-start | bytes 589832 | tf_op jit(solution)/shard_map/ppermute | solution.py:432
  61.5 12.7 %collective-permute-done.2.refs_1_ = bf16[96,1024]{1,0:T(8,128)(2,1)S(1)} collective-permute-done((bf16[96,1024]{1,0:T(8,128)(2,1)S(1)}, bf16[96,1024]{1,0:T(8,128)(2,1)S(1)}, u32[]{:S(2)}, u32[]{:S(2)}) %collective-permute-start.2) | collective-permute-done | bytes 196640 | tf_op jit(solution)/shard_map/ppermute | solution.py:432
  74.2 1.9 %collective-permute-start.3 = (bf16[96,1024]{1,0:T(8,128)(2,1)S(1)}, bf16[96,1024]{1,0:T(8,128)(2,1)S(1)}, u32[]{:S(2)}, u32[]{:S(2)}) collective-permute-start(bf16[96,1024]{1,0:T(8,128)(2,1)S(1)} %collective-permute-done.2.refs_1_), channel_id=1, source_target_pairs={{0,4},{4,0},{1,5},{5,1},{2,6},{6,2},{3,7},{7,3},{8,12},{12,8},{9,1... | collective-permute-start | bytes 589832 | tf_op jit(solution)/shard_map/ppermute | solution.py:432
  76.1 1.4 %collective-permute-done.3.refs_2_ = bf16[96,1024]{1,0:T(8,128)(2,1)S(1)} collective-permute-done((bf16[96,1024]{1,0:T(8,128)(2,1)S(1)}, bf16[96,1024]{1,0:T(8,128)(2,1)S(1)}, u32[]{:S(2)}, u32[]{:S(2)}) %collective-permute-start.3) | collective-permute-done | bytes 196640 | tf_op jit(solution)/shard_map/ppermute | solution.py:432
  77.6 0.7 copy-done.8
  78.2 1.5 %shard_map.219 = (bf16[3456,256]{1,0:T(8,128)(2,1)S(1)}, bf16[96,1024]{1,0:T(8,128)(2,1)S(1)}, bf16[96,1024]{1,0:T(8,128)(2,1)S(1)}) custom-call(bf16[3456,256]{1,0:T(8,128)(2,1)} %collective-permute-done.1.refs_0_, bf16[96,1024]{1,0:T(8,128)(2,1)} %copy-done.7, bf16[96,1024]{1,0:T(8,128)(2,1)} %copy-done.8), custom_call_target="tpu_custom_call" | custom-call | tf_op jit(solution)/shard_map/pallas_call | solution.py:548
  79.8 3.5 %shard_map.220 = bf16[512,512]{1,0:T(8,128)(2,1)} custom-call(bf16[512,512]{1,0:T(8,128)(2,1)S(1)} %bitcast.14, bf16[3456,256]{1,0:T(8,128)(2,1)} %shard_map.218.own_hbm, bf16[3456,256]{1,0:T(8,128)(2,1)S(1)} %get-tuple-element.28.sib, bf16[96,1024]{1,0:T(8,128)(2,1)S(1)} %get-tuple-element.29.dense_y, bf16[96,1024]{1,0:T(8,128)(2,1)S(1)} %get-tuple-element.30.dense_yc), custom_call_target="tpu_custom_call" | custom-call | tf_op jit(solution)/shard_map/pallas_call | solution.py:555
  83.3 12.8 %all-to-all-start.3 = ((bf16[64,8,512]{2,1,0:T(8,128)(2,1)}), bf16[64,8,512]{2,1,0:T(8,128)(2,1)S(1)}, u32[]{:S(2)}, u32[]{:S(2)}) async-start(bf16[64,8,512]{2,1,0:T(8,128)(2,1)} %bitcast.19), calls=%async_computation.3 | async-start | bytes 1048576 | tf_op jit(solution)/shard_map/all_to_all | solution.py:428
  96.3 19.2 %all-to-all-done.3 = bf16[64,8,512]{2,1,0:T(8,128)(2,1)S(1)} async-done(((bf16[64,8,512]{2,1,0:T(8,128)(2,1)}), bf16[64,8,512]{2,1,0:T(8,128)(2,1)S(1)}, u32[]{:S(2)}, u32[]{:S(2)}) %all-to-all-start.3) | async-done | bytes 524320 | tf_op jit(solution)/shard_map/all_to_all | solution.py:428
  115.6 0.9 shard_map.221
  116.5 3.3 %all-to-all-start.4 = ((bf16[4,8,512]{2,1,0:T(8,128)(2,1)}), bf16[4,8,512]{2,1,0:T(8,128)(2,1)S(1)}, u32[]{:S(2)}, u32[]{:S(2)}) async-start(bf16[4,8,512]{2,1,0:T(8,128)(2,1)} %bitcast.13), calls=%async_computation.4 | async-start | bytes 65536 | tf_op jit(solution)/shard_map/all_to_all | solution.py:428
  119.8 0.8 shard_map.223
  120.5 4.6 %all-to-all-done.4.parts = bf16[4,8,512]{2,1,0:T(8,128)(2,1)S(1)} async-done(((bf16[4,8,512]{2,1,0:T(8,128)(2,1)}), bf16[4,8,512]{2,1,0:T(8,128)(2,1)S(1)}, u32[]{:S(2)}, u32[]{:S(2)}) %all-to-all-start.4) | async-done | bytes 32800 | tf_op jit(solution)/shard_map/all_to_all | solution.py:428
  125.2 0.6 shard_map.222
  (32 shorter events, 0.4 us)
Async XLA Ops:
  22.3 4.4 %copy-start.5 = (bf16[4,1032,128]{2,1,0:T(8,128)(2,1)}, bf16[4,1032,128]{2,1,0:T(8,128)(2,1)S(1)}, u32[]{:S(2)}) copy-start(bf16[4,1032,128]{2,1,0:T(8,128)(2,1)S(1)} %all_to_all.25.own_hbm) | copy-start | bytes 3170308
  22.3 8.9 %collective-permute-start = (bf16[4,1032,128]{2,1,0:T(8,128)(2,1)S(1)}, bf16[4,1032,128]{2,1,0:T(8,128)(2,1)S(1)}, u32[]{:S(2)}, u32[]{:S(2)}) collective-permute-start(bf16[4,1032,128]{2,1,0:T(8,128)(2,1)S(1)} %all_to_all.25.own_hbm), channel_id=1, source_target_pairs={{0,4},{4,0},{1,5},{5,1},{2,6},{6,2},{3,7},{7,3},{8,12},{12,8},{9,1... | collective-permute-start | bytes 3170312 | tf_op jit(solution)/shard_map/ppermute | solution.py:432
  24.2 4.9 %copy-start.9 = (bf16[1024]{0:T(1024)(128)(2,1)S(1)}, bf16[1024]{0:T(1024)(128)(2,1)}, u32[]{:S(2)}) copy-start(bf16[1024]{0:T(1024)(128)(2,1)} %param.21) | copy-start | bytes 6148
  24.2 4.9 %copy-start.10 = (bf16[1024]{0:T(1024)(128)(2,1)S(1)}, bf16[1024]{0:T(1024)(128)(2,1)}, u32[]{:S(2)}) copy-start(bf16[1024]{0:T(1024)(128)(2,1)} %param.22) | copy-start | bytes 6148
  24.2 4.9 %copy-start.2 = (bf16[4,1024]{1,0:T(4,128)(2,1)S(1)}, bf16[4,1024]{1,0:T(4,128)(2,1)}, u32[]{:S(2)}) copy-start(bf16[4,1024]{1,0:T(4,128)(2,1)} %tokens.3) | copy-start | bytes 24580
  26.7 50.9 %collective-permute-start.1 = (bf16[3456,256]{1,0:T(8,128)(2,1)}, bf16[3456,256]{1,0:T(8,128)(2,1)}, u32[]{:S(2)}, u32[]{:S(2)}) collective-permute-start(bf16[3456,256]{1,0:T(8,128)(2,1)} %shard_map.218.own_hbm), channel_id=1, source_target_pairs={{0,4},{4,0},{1,5},{5,1},{2,6},{6,2},{3,7},{7,3},{8,12},{12,8},{9,1... | collective-permute-start | bytes 5308424 | tf_op jit(solution)/shard_map/ppermute | solution.py:432
  29.2 2.0 %copy-start.3 = (s32[4]{0:T(128)S(1)}, s32[4]{0:T(128)}, u32[]{:S(2)}) copy-start(s32[4]{0:T(128)} %lengths.1) | copy-start | bytes 52
  29.2 2.0 %copy-start.4 = (f32[8]{0:T(128)S(1)}, f32[8]{0:T(128)}, u32[]{:S(2)}) copy-start(f32[8]{0:T(128)} %param.27) | copy-start | bytes 100
  33.6 25.6 %copy-start.6 = (bf16[96,1024]{1,0:T(8,128)(2,1)S(1)}, bf16[96,1024]{1,0:T(8,128)(2,1)}, u32[]{:S(2)}) copy-start(bf16[96,1024]{1,0:T(8,128)(2,1)} %get-tuple-element.27.dense) | copy-start | bytes 589828
  42.5 37.2 %all-to-all-start.2 = ((bf16[64,8,512]{2,1,0:T(8,128)(2,1)}), bf16[64,8,512]{2,1,0:T(8,128)(2,1)S(1)}, u32[]{:S(2)}, u32[]{:S(2)}) async-start(bf16[64,8,512]{2,1,0:T(8,128)(2,1)} %bitcast.20), calls=%async_computation.2 | async-start | bytes 1048576 | tf_op jit(solution)/shard_map/all_to_all | solution.py:428
  59.2 15.1 %collective-permute-start.2 = (bf16[96,1024]{1,0:T(8,128)(2,1)S(1)}, bf16[96,1024]{1,0:T(8,128)(2,1)S(1)}, u32[]{:S(2)}, u32[]{:S(2)}) collective-permute-start(bf16[96,1024]{1,0:T(8,128)(2,1)S(1)} %copy-done.6), channel_id=1, source_target_pairs={{0,8},{8,0},{16,24},{24,16},{32,40},{40,32},{48,56},{56,48},{1,9},... | collective-permute-start | bytes 589832 | tf_op jit(solution)/shard_map/ppermute | solution.py:432
  74.2 3.3 %copy-start.7 = (bf16[96,1024]{1,0:T(8,128)(2,1)}, bf16[96,1024]{1,0:T(8,128)(2,1)S(1)}, u32[]{:S(2)}) copy-start(bf16[96,1024]{1,0:T(8,128)(2,1)S(1)} %collective-permute-done.2.refs_1_) | copy-start | bytes 589828
  74.2 3.3 %collective-permute-start.3 = (bf16[96,1024]{1,0:T(8,128)(2,1)S(1)}, bf16[96,1024]{1,0:T(8,128)(2,1)S(1)}, u32[]{:S(2)}, u32[]{:S(2)}) collective-permute-start(bf16[96,1024]{1,0:T(8,128)(2,1)S(1)} %collective-permute-done.2.refs_1_), channel_id=1, source_target_pairs={{0,4},{4,0},{1,5},{5,1},{2,6},{6,2},{3,7},{7,3},{8,12},{12,8},{9,1... | collective-permute-start | bytes 589832 | tf_op jit(solution)/shard_map/ppermute | solution.py:432
  77.5 0.7 copy-start.8
  79.8 16.3 %copy-start.11 = (bf16[1024]{0:T(1024)(128)(2,1)S(1)}, bf16[1024]{0:T(1024)(128)(2,1)}, u32[]{:S(2)}) copy-start(bf16[1024]{0:T(1024)(128)(2,1)} %param.34) | copy-start | bytes 6148
  83.3 36.5 %copy-start = (bf16[1024,128]{1,0:T(8,128)(2,1)S(1)}, bf16[1024,128]{1,0:T(8,128)(2,1)}, u32[]{:S(2)}) copy-start(bf16[1024,128]{1,0:T(8,128)(2,1)} %wk.1) | copy-start | bytes 786436
  83.3 36.5 %copy-start.1 = (bf16[1024,128]{1,0:T(8,128)(2,1)S(1)}, bf16[1024,128]{1,0:T(8,128)(2,1)}, u32[]{:S(2)}) copy-start(bf16[1024,128]{1,0:T(8,128)(2,1)} %wv.1) | copy-start | bytes 786436
  83.3 32.3 %all-to-all-start.3 = ((bf16[64,8,512]{2,1,0:T(8,128)(2,1)}), bf16[64,8,512]{2,1,0:T(8,128)(2,1)S(1)}, u32[]{:S(2)}, u32[]{:S(2)}) async-start(bf16[64,8,512]{2,1,0:T(8,128)(2,1)} %bitcast.19), calls=%async_computation.3 | async-start | bytes 1048576 | tf_op jit(solution)/shard_map/all_to_all | solution.py:428
  116.5 8.7 %all-to-all-start.4 = ((bf16[4,8,512]{2,1,0:T(8,128)(2,1)}), bf16[4,8,512]{2,1,0:T(8,128)(2,1)S(1)}, u32[]{:S(2)}, u32[]{:S(2)}) async-start(bf16[4,8,512]{2,1,0:T(8,128)(2,1)} %bitcast.13), calls=%async_computation.4 | async-start | bytes 65536 | tf_op jit(solution)/shard_map/all_to_all | solution.py:428

commit v2 on v1

--- a/solution.py
+++ b/solution.py
@@ -177,9 +177,9 @@
     a = attn_in[...].astype(F32)
     x_own = ordered(a[:, :HALF], a[:, HALF:]).astype(BF16)
     x_sib = ordered(a[:, HALF:], a[:, :HALF]).astype(BF16)
-    q = jnp.concatenate(
-        [dot(x_own, w_own[t, 0:HALF, :]) + dot(x_sib, w_sib[t, 0:HALF, :]) for t in range(TP)],
-        axis=1,
+    q = sum(
+        dot(a, jnp.concatenate([w[t, 0:HALF, :] for t in range(TP)], axis=1))
+        for a, w in ((x_own, w_own), (x_sib, w_sib))
     )
     q = q.astype(BF16).astype(F32)
     head_mask = iota((HEADS, HEADS * HEAD), 1) // HEAD == iota((HEADS, HEADS * HEAD), 0)
@@ -241,14 +241,11 @@
     ).astype(BF16)
 
     def project(w):
-        parts = []
-        for j in range(4):
-            row = HALF + 128 * j
-            acc = dot(mixed[:, 0:128], w[0, row : row + 128, :])
-            for t in range(1, TP):
-                acc = acc + dot(mixed[:, 128 * t : 128 * t + 128], w[t, row : row + 128, :])
-            parts.append(acc)
-        return jnp.concatenate(parts, axis=1)
+        rows = [
+            jnp.concatenate([w[t, HALF + 128 * j : HALF + 128 * (j + 1), :] for j in range(4)], axis=1)
+            for t in range(TP)
+        ]
+        return dot(mixed, jnp.concatenate(rows, axis=0))
 
     out_own, out_sib = project(w_own), project(w_sib)
     total = jnp.concatenate([ordered(out_own, out_sib), ordered(out_sib, out_own)], axis=1)

time: 126 us -> 126 us (level)
  no operation moved by 1% of the time
where the time goes in v2:
time: 126 us
  starting transfers between devices  41.2 us (33%)
  waiting for transfers between devices  38 us (30%)
  blocking collectives  27.4 us (22%)
  Pallas kernels  17.3 us (14%)
    all_to_all x3, starting transfers between devices, a2a(): return lax.all_to_all(array, axis, split_axis=0, concat_axis=0, tiled=True)  32.6 us
    all_to_all x2, blocking collectives, a2a(): return lax.all_to_all(array, axis, split_axis=0, concat_axis=0, tiled=True)  27.4 us
    all_to_all x3, waiting for transfers between devices, a2a(): return lax.all_to_all(array, axis, split_axis=0, concat_axis=0, tiled=True)  23.9 us
    ppermute x4, waiting for transfers between devices, swap(): lax.ppermute(array, axis, [(i, i ^ 1) for i in range(lax.axis_size(axis))])  14.1 us
    ppermute x4, starting transfers between devices, swap(): lax.ppermute(array, axis, [(i, i ^ 1) for i in range(lax.axis_size(axis))])  8.59 us
    pallas_call x1, Pallas kernels, body(): call(expert_kernel, pltpu.HBM((ROWS, HALF), BF16), [VMEM, HBM] + [VMEM] *...  3.48 us
  transfers between devices with their start and end apart: 7, of which 4 were waited for; matrix products, arithmetic and copies ran while one was open for 0% of the time, Pallas kernels for 8%

profile of v2, /device:TPU:8, one launch (start us, length us, event | category | flops | bytes accessed | tf_op | source)
XLA Modules:
  0.0 125.6 jit_solution(14720591398379695671)
XLA Ops:
  0.6 2.1 %shard_map.212 = (bf16[4,1032,128]{2,1,0:T(8,128)(2,1)}, bf16[96,1024]{1,0:T(8,128)(2,1)}) custom-call(s32[1]{0:T(128)} %bitcast.core, bf16[1024,128]{1,0:T(8,128)(2,1)} %wq.1, bf16[128,1024]{1,0:T(8,128)(2,1)} %wo.1, s32[2,4]{1,0:T(2,128)} %bitcast.24, f32[2,4]{1,0:T(2,128)} %bitcast.25, bf16[32,1024]{1,0:T(8,128)(2,1)} %gate.1, bf16[32,1024]{1,0:T(8,128)(2,1)} %up.1, ...), custom_call_target="tpu_custom_call" | custom-call | tf_op jit(solution)/shard_map/pallas_call | solution.py:457
  2.8 19.5 %all_to_all.25.own_hbm = bf16[4,1032,128]{2,1,0:T(8,128)(2,1)S(1)} all-to-all(bf16[4,1032,128]{2,1,0:T(8,128)(2,1)} %get-tuple-element.18), channel_id=1, replica_groups=mesh['z'=8,'y'=8,'c'=2,'x'=4] {'x'}, dimensions={0} | all-to-all | bytes 2113536 | tf_op jit(solution)/shard_map/all_to_all | solution.py:425
  22.3 1.9 %collective-permute-start = (bf16[4,1032,128]{2,1,0:T(8,128)(2,1)S(1)}, bf16[4,1032,128]{2,1,0:T(8,128)(2,1)S(1)}, u32[]{:S(2)}, u32[]{:S(2)}) collective-permute-start(bf16[4,1032,128]{2,1,0:T(8,128)(2,1)S(1)} %all_to_all.25.own_hbm), channel_id=1, source_target_pairs={{0,4},{4,0},{1,5},{5,1},{2,6},{6,2},{3,7},{7,3},{8,12},{12,8},{9,1... | collective-permute-start | bytes 3170312 | tf_op jit(solution)/shard_map/ppermute | solution.py:429
  24.2 2.4 %shard_map.218.own_hbm = bf16[3456,256]{1,0:T(8,128)(2,1)} custom-call(bf16[1024,256]{1,0:T(8,128)(2,1)} %bitcast.21, bf16[1024,256]{1,0:T(8,128)(2,1)} %bitcast.22, bf16[256,1024]{1,0:T(8,128)(2,1)} %bitcast.23, bf16[96,1024]{1,0:T(8,128)(2,1)} %get-tuple-element.27.dense), custom_call_target="tpu_custom_call" | custom-call | tf_op jit(solution)/shard_map/pallas_call | solution.py:482
  26.7 2.4 %collective-permute-start.1 = (bf16[3456,256]{1,0:T(8,128)(2,1)}, bf16[3456,256]{1,0:T(8,128)(2,1)}, u32[]{:S(2)}, u32[]{:S(2)}) collective-permute-start(bf16[3456,256]{1,0:T(8,128)(2,1)} %shard_map.218.own_hbm), channel_id=1, source_target_pairs={{0,4},{4,0},{1,5},{5,1},{2,6},{6,2},{3,7},{7,3},{8,12},{12,8},{9,1... | collective-permute-start | bytes 5308424 | tf_op jit(solution)/shard_map/ppermute | solution.py:429
  29.3 2.0 %shard_map.213 = (bf16[512,32]{1,0:T(8,128)(2,1)S(1)}, f32[32,512]{1,0:T(8,128)S(1)}, f32[32,512]{1,0:T(8,128)S(1)}, bf16[4,1032,128]{2,1,0:T(8,128)(2,1)S(1)}, ...) custom-call(s32[1]{0:T(128)} %bitcast.1.tp, bf16[4,1032,128]{2,1,0:T(8,128)(2,1)} %copy-done.5, ...), custom_call_target="tpu_custom_call" | custom-call | tf_op jit(solution)/shard_map/pallas_call | solution.py:501
  31.2 2.2 %shard_map.214 = (bf16[4,1024]{1,0:T(4,128)(2,1)S(1)}, bf16[4,8,512]{2,1,0:T(8,128)(2,1)S(1)}) custom-call(s32[1]{0:T(128)} %bitcast.core, s32[4]{0:T(128)S(1)} %copy-done.3, bf16[4,1024]{1,0:T(4,128)(2,1)S(1)} %copy-done.2, bf16[4,1024]{1,0:T(4,128)(2,1)S(1)} %shard_map.211.attn_in, bf16[4,1032,128]{2,1,0:T(8,128)(2,1)S(1)} %get-tuple-element.19.w_own, ...), custom_call_target="tpu_custom_call" | custom-call | tf_op jit(solution)/shard_map/pallas_call | solution.py:514
  33.4 7.9 %all_to_all.26 = bf16[4,8,512]{2,1,0:T(8,128)(2,1)S(1)} all-to-all(bf16[4,8,512]{2,1,0:T(8,128)(2,1)S(1)} %get-tuple-element.23), channel_id=1, replica_groups=mesh['z'=8,'y'=8,'c'=2,'x'=4] {'x'}, dimensions={0} | all-to-all | bytes 65536 | tf_op jit(solution)/shard_map/all_to_all | solution.py:425
  41.4 1.0 shard_map.217
  42.4 16.6 %all-to-all-start.2 = ((bf16[64,8,512]{2,1,0:T(8,128)(2,1)}), bf16[64,8,512]{2,1,0:T(8,128)(2,1)S(1)}, u32[]{:S(2)}, u32[]{:S(2)}) async-start(bf16[64,8,512]{2,1,0:T(8,128)(2,1)} %bitcast.20), calls=%async_computation.2 | async-start | bytes 1048576 | tf_op jit(solution)/shard_map/all_to_all | solution.py:425
  59.0 2.4 %collective-permute-start.2 = (bf16[96,1024]{1,0:T(8,128)(2,1)S(1)}, bf16[96,1024]{1,0:T(8,128)(2,1)S(1)}, u32[]{:S(2)}, u32[]{:S(2)}) collective-permute-start(bf16[96,1024]{1,0:T(8,128)(2,1)S(1)} %copy-done.6), channel_id=1, source_target_pairs={{0,8},{8,0},{16,24},{24,16},{32,40},{40,32},{48,56},{56,48},{1,9},... | collective-permute-start | bytes 589832 | tf_op jit(solution)/shard_map/ppermute | solution.py:429
  61.4 12.7 %collective-permute-done.2.refs_1_ = bf16[96,1024]{1,0:T(8,128)(2,1)S(1)} collective-permute-done((bf16[96,1024]{1,0:T(8,128)(2,1)S(1)}, bf16[96,1024]{1,0:T(8,128)(2,1)S(1)}, u32[]{:S(2)}, u32[]{:S(2)}) %collective-permute-start.2) | collective-permute-done | bytes 196640 | tf_op jit(solution)/shard_map/ppermute | solution.py:429
  74.1 1.9 %collective-permute-start.3 = (bf16[96,1024]{1,0:T(8,128)(2,1)S(1)}, bf16[96,1024]{1,0:T(8,128)(2,1)S(1)}, u32[]{:S(2)}, u32[]{:S(2)}) collective-permute-start(bf16[96,1024]{1,0:T(8,128)(2,1)S(1)} %collective-permute-done.2.refs_1_), channel_id=1, source_target_pairs={{0,4},{4,0},{1,5},{5,1},{2,6},{6,2},{3,7},{7,3},{8,12},{12,8},{9,1... | collective-permute-start | bytes 589832 | tf_op jit(solution)/shard_map/ppermute | solution.py:429
  76.0 1.4 %collective-permute-done.3.refs_2_ = bf16[96,1024]{1,0:T(8,128)(2,1)S(1)} collective-permute-done((bf16[96,1024]{1,0:T(8,128)(2,1)S(1)}, bf16[96,1024]{1,0:T(8,128)(2,1)S(1)}, u32[]{:S(2)}, u32[]{:S(2)}) %collective-permute-start.3) | collective-permute-done | bytes 196640 | tf_op jit(solution)/shard_map/ppermute | solution.py:429
  77.4 0.7 copy-done.8
  78.1 1.5 %shard_map.219 = (bf16[3456,256]{1,0:T(8,128)(2,1)S(1)}, bf16[96,1024]{1,0:T(8,128)(2,1)S(1)}, bf16[96,1024]{1,0:T(8,128)(2,1)S(1)}) custom-call(bf16[3456,256]{1,0:T(8,128)(2,1)} %collective-permute-done.1.refs_0_, bf16[96,1024]{1,0:T(8,128)(2,1)} %copy-done.7, bf16[96,1024]{1,0:T(8,128)(2,1)} %copy-done.8), custom_call_target="tpu_custom_call" | custom-call | tf_op jit(solution)/shard_map/pallas_call | solution.py:545
  79.6 3.5 %shard_map.220 = bf16[512,512]{1,0:T(8,128)(2,1)} custom-call(bf16[512,512]{1,0:T(8,128)(2,1)S(1)} %bitcast.14, bf16[3456,256]{1,0:T(8,128)(2,1)} %shard_map.218.own_hbm, bf16[3456,256]{1,0:T(8,128)(2,1)S(1)} %get-tuple-element.28.sib, bf16[96,1024]{1,0:T(8,128)(2,1)S(1)} %get-tuple-element.29.dense_y, bf16[96,1024]{1,0:T(8,128)(2,1)S(1)} %get-tuple-element.30.dense_yc), custom_call_target="tpu_custom_call" | custom-call | tf_op jit(solution)/shard_map/pallas_call | solution.py:552
  83.1 12.8 %all-to-all-start.3 = ((bf16[64,8,512]{2,1,0:T(8,128)(2,1)}), bf16[64,8,512]{2,1,0:T(8,128)(2,1)S(1)}, u32[]{:S(2)}, u32[]{:S(2)}) async-start(bf16[64,8,512]{2,1,0:T(8,128)(2,1)} %bitcast.19), calls=%async_computation.3 | async-start | bytes 1048576 | tf_op jit(solution)/shard_map/all_to_all | solution.py:425
  96.2 19.2 %all-to-all-done.3 = bf16[64,8,512]{2,1,0:T(8,128)(2,1)S(1)} async-done(((bf16[64,8,512]{2,1,0:T(8,128)(2,1)}), bf16[64,8,512]{2,1,0:T(8,128)(2,1)S(1)}, u32[]{:S(2)}, u32[]{:S(2)}) %all-to-all-start.3) | async-done | bytes 524320 | tf_op jit(solution)/shard_map/all_to_all | solution.py:425
  115.4 0.9 shard_map.221
  116.3 3.3 %all-to-all-start.4 = ((bf16[4,8,512]{2,1,0:T(8,128)(2,1)}), bf16[4,8,512]{2,1,0:T(8,128)(2,1)S(1)}, u32[]{:S(2)}, u32[]{:S(2)}) async-start(bf16[4,8,512]{2,1,0:T(8,128)(2,1)} %bitcast.13), calls=%async_computation.4 | async-start | bytes 65536 | tf_op jit(solution)/shard_map/all_to_all | solution.py:425
  119.6 0.8 shard_map.223
  120.4 4.6 %all-to-all-done.4.parts = bf16[4,8,512]{2,1,0:T(8,128)(2,1)S(1)} async-done(((bf16[4,8,512]{2,1,0:T(8,128)(2,1)}), bf16[4,8,512]{2,1,0:T(8,128)(2,1)S(1)}, u32[]{:S(2)}, u32[]{:S(2)}) %all-to-all-start.4) | async-done | bytes 32800 | tf_op jit(solution)/shard_map/all_to_all | solution.py:425
  125.0 0.6 shard_map.222
  (32 shorter events, 0.4 us)
Async XLA Ops:
  22.3 4.4 %copy-start.5 = (bf16[4,1032,128]{2,1,0:T(8,128)(2,1)}, bf16[4,1032,128]{2,1,0:T(8,128)(2,1)S(1)}, u32[]{:S(2)}) copy-start(bf16[4,1032,128]{2,1,0:T(8,128)(2,1)S(1)} %all_to_all.25.own_hbm) | copy-start | bytes 3170308
  22.3 8.9 %collective-permute-start = (bf16[4,1032,128]{2,1,0:T(8,128)(2,1)S(1)}, bf16[4,1032,128]{2,1,0:T(8,128)(2,1)S(1)}, u32[]{:S(2)}, u32[]{:S(2)}) collective-permute-start(bf16[4,1032,128]{2,1,0:T(8,128)(2,1)S(1)} %all_to_all.25.own_hbm), channel_id=1, source_target_pairs={{0,4},{4,0},{1,5},{5,1},{2,6},{6,2},{3,7},{7,3},{8,12},{12,8},{9,1... | collective-permute-start | bytes 3170312 | tf_op jit(solution)/shard_map/ppermute | solution.py:429
  24.2 4.9 %copy-start.9 = (bf16[1024]{0:T(1024)(128)(2,1)S(1)}, bf16[1024]{0:T(1024)(128)(2,1)}, u32[]{:S(2)}) copy-start(bf16[1024]{0:T(1024)(128)(2,1)} %param.21) | copy-start | bytes 6148
  24.2 4.9 %copy-start.10 = (bf16[1024]{0:T(1024)(128)(2,1)S(1)}, bf16[1024]{0:T(1024)(128)(2,1)}, u32[]{:S(2)}) copy-start(bf16[1024]{0:T(1024)(128)(2,1)} %param.22) | copy-start | bytes 6148
  24.2 4.9 %copy-start.2 = (bf16[4,1024]{1,0:T(4,128)(2,1)S(1)}, bf16[4,1024]{1,0:T(4,128)(2,1)}, u32[]{:S(2)}) copy-start(bf16[4,1024]{1,0:T(4,128)(2,1)} %tokens.3) | copy-start | bytes 24580
  26.7 50.7 %collective-permute-start.1 = (bf16[3456,256]{1,0:T(8,128)(2,1)}, bf16[3456,256]{1,0:T(8,128)(2,1)}, u32[]{:S(2)}, u32[]{:S(2)}) collective-permute-start(bf16[3456,256]{1,0:T(8,128)(2,1)} %shard_map.218.own_hbm), channel_id=1, source_target_pairs={{0,4},{4,0},{1,5},{5,1},{2,6},{6,2},{3,7},{7,3},{8,12},{12,8},{9,1... | collective-permute-start | bytes 5308424 | tf_op jit(solution)/shard_map/ppermute | solution.py:429
  29.2 2.0 %copy-start.3 = (s32[4]{0:T(128)S(1)}, s32[4]{0:T(128)}, u32[]{:S(2)}) copy-start(s32[4]{0:T(128)} %lengths.1) | copy-start | bytes 52
  29.2 2.0 %copy-start.4 = (f32[8]{0:T(128)S(1)}, f32[8]{0:T(128)}, u32[]{:S(2)}) copy-start(f32[8]{0:T(128)} %param.27) | copy-start | bytes 100
  33.4 25.6 %copy-start.6 = (bf16[96,1024]{1,0:T(8,128)(2,1)S(1)}, bf16[96,1024]{1,0:T(8,128)(2,1)}, u32[]{:S(2)}) copy-start(bf16[96,1024]{1,0:T(8,128)(2,1)} %get-tuple-element.27.dense) | copy-start | bytes 589828
  42.4 37.2 %all-to-all-start.2 = ((bf16[64,8,512]{2,1,0:T(8,128)(2,1)}), bf16[64,8,512]{2,1,0:T(8,128)(2,1)S(1)}, u32[]{:S(2)}, u32[]{:S(2)}) async-start(bf16[64,8,512]{2,1,0:T(8,128)(2,1)} %bitcast.20), calls=%async_computation.2 | async-start | bytes 1048576 | tf_op jit(solution)/shard_map/all_to_all | solution.py:425
  59.0 15.1 %collective-permute-start.2 = (bf16[96,1024]{1,0:T(8,128)(2,1)S(1)}, bf16[96,1024]{1,0:T(8,128)(2,1)S(1)}, u32[]{:S(2)}, u32[]{:S(2)}) collective-permute-start(bf16[96,1024]{1,0:T(8,128)(2,1)S(1)} %copy-done.6), channel_id=1, source_target_pairs={{0,8},{8,0},{16,24},{24,16},{32,40},{40,32},{48,56},{56,48},{1,9},... | collective-permute-start | bytes 589832 | tf_op jit(solution)/shard_map/ppermute | solution.py:429
  74.1 3.3 %copy-start.7 = (bf16[96,1024]{1,0:T(8,128)(2,1)}, bf16[96,1024]{1,0:T(8,128)(2,1)S(1)}, u32[]{:S(2)}) copy-start(bf16[96,1024]{1,0:T(8,128)(2,1)S(1)} %collective-permute-done.2.refs_1_) | copy-start | bytes 589828
  74.1 3.3 %collective-permute-start.3 = (bf16[96,1024]{1,0:T(8,128)(2,1)S(1)}, bf16[96,1024]{1,0:T(8,128)(2,1)S(1)}, u32[]{:S(2)}, u32[]{:S(2)}) collective-permute-start(bf16[96,1024]{1,0:T(8,128)(2,1)S(1)} %collective-permute-done.2.refs_1_), channel_id=1, source_target_pairs={{0,4},{4,0},{1,5},{5,1},{2,6},{6,2},{3,7},{7,3},{8,12},{12,8},{9,1... | collective-permute-start | bytes 589832 | tf_op jit(solution)/shard_map/ppermute | solution.py:429
  77.4 0.7 copy-start.8
  79.6 16.3 %copy-start.11 = (bf16[1024]{0:T(1024)(128)(2,1)S(1)}, bf16[1024]{0:T(1024)(128)(2,1)}, u32[]{:S(2)}) copy-start(bf16[1024]{0:T(1024)(128)(2,1)} %param.34) | copy-start | bytes 6148
  83.1 36.5 %copy-start = (bf16[1024,128]{1,0:T(8,128)(2,1)S(1)}, bf16[1024,128]{1,0:T(8,128)(2,1)}, u32[]{:S(2)}) copy-start(bf16[1024,128]{1,0:T(8,128)(2,1)} %wk.1) | copy-start | bytes 786436
  83.1 36.5 %copy-start.1 = (bf16[1024,128]{1,0:T(8,128)(2,1)S(1)}, bf16[1024,128]{1,0:T(8,128)(2,1)}, u32[]{:S(2)}) copy-start(bf16[1024,128]{1,0:T(8,128)(2,1)} %wv.1) | copy-start | bytes 786436
  83.1 32.3 %all-to-all-start.3 = ((bf16[64,8,512]{2,1,0:T(8,128)(2,1)}), bf16[64,8,512]{2,1,0:T(8,128)(2,1)S(1)}, u32[]{:S(2)}, u32[]{:S(2)}) async-start(bf16[64,8,512]{2,1,0:T(8,128)(2,1)} %bitcast.19), calls=%async_computation.3 | async-start | bytes 1048576 | tf_op jit(solution)/shard_map/all_to_all | solution.py:425
  116.3 8.7 %all-to-all-start.4 = ((bf16[4,8,512]{2,1,0:T(8,128)(2,1)}), bf16[4,8,512]{2,1,0:T(8,128)(2,1)S(1)}, u32[]{:S(2)}, u32[]{:S(2)}) async-start(bf16[4,8,512]{2,1,0:T(8,128)(2,1)} %bitcast.13), calls=%async_computation.4 | async-start | bytes 65536 | tf_op jit(solution)/shard_map/all_to_all | solution.py:425

commit v3 on v2

--- a/solution.py
+++ b/solution.py
@@ -19,6 +19,10 @@
 TP = 4
 CHIPS = 64
 MSG = 8
+BLK = 8
+SLOTS = 3
+WIDE = SLOTS * 128
+TOK = TP * BLK * 4
 ROWS = CHIPS * MSG
 F32 = jnp.float32
 BF16 = jnp.bfloat16
@@ -144,6 +148,11 @@
         b.start()
     for c in outs:
         c.wait()
+
+
+def join_kernel(a, b, c, out):
+    for n, ref in enumerate((a, b, c)):
+        out[DENSE_ROWS * n : DENSE_ROWS * (n + 1), :] = ref[...]
 
 
 def fetch_kernel(*refs):
@@ -252,14 +261,28 @@
     res = (tokens[...].astype(F32) + total).astype(BF16)
     residual[...] = res
     f = rms(res, gain[...])
-    f = jnp.concatenate([f[:, :HALF], f[:, HALF:]], axis=0).astype(BF16)
+    f = jnp.concatenate([f[:, 128 * k : 128 * (k + 1)] for k in range(BLK)], axis=0).astype(BF16)
     for d in range(TP):
         sent[d] = f
 
 
-def table_kernel(
-    tp, own_hbm, keys_hbm, values_hbm, pick, weight, mine_out, own, keys, values, sems
-):
+def parts_of(token, place):
+    same = (token // 4) % BLK == place % BLK
+    chip = place // BLK
+    return same, chip, token // 32, token % 4
+
+
+def is_mine(tp, same, chip, t, i):
+    return same & (t == tp) & (i == 2 * ((chip // 8) % 2) + chip % 2)
+
+
+def before(first, second):
+    return (
+        ((first // 4) % BLK == 0) & (first // 32 * 4 + first % 4 < second // 32 * 4 + second % 4)
+    ).astype(F32).astype(BF16)
+
+
+def table_kernel(tp, own_hbm, keys_hbm, values_hbm, pick, info, own, keys, values, sems):
     copies = [
         [pltpu.make_async_copy(src.at[b], dst.at[b], sems.at[k, b]) for b in range(OWN)]
         for k, (src, dst) in enumerate(((own_hbm, own), (keys_hbm, keys), (values_hbm, values)))
@@ -269,53 +292,79 @@
             c.start()
     for c in copies[0]:
         c.wait()
-    n = TP * 8
-    row, col = iota((n, ROWS), 0), iota((n, ROWS), 1)
-    facts = jnp.concatenate([own[t, 2 * HALF :, :] for t in range(TP)], axis=0).astype(F32)
+    facts = jnp.concatenate(
+        [own[t, 2 * HALF :, :].astype(F32) for t in range(TP) for _ in range(BLK // 2)], axis=0
+    )
+    info[...] = facts
+    eye = iota((TOK, TOK), 0) == iota((TOK, TOK), 1)
+    id0, id1 = (
+        jnp.sum(jnp.where(eye, facts[:, n : n + 1], 0.0), axis=0, keepdims=True) for n in range(2)
+    )
+    token, place = iota((ROWS, TOK), 1), iota((ROWS, TOK), 0)
+    same, chip, t, i = parts_of(token, place)
+    expert = (chip // 2).astype(F32)
+    chosen = jnp.where((id0 == expert) | (id1 == expert), 1.0, 0.0)
+    earlier = dot(chosen.astype(BF16), before(iota((TOK, TOK), 0), iota((TOK, TOK), 1)))
+    kept = jnp.where(same, chosen, 0.0)
+    for r in range(2):
+        pick[r] = jnp.where(earlier == float(r), kept, 0.0).astype(BF16)
+    pick[2] = jnp.where(is_mine(tp[0], same, chip, t, i), 1.0, 0.0).astype(BF16)
+    for group in copies[1:]:
+        for c in group:
+            c.wait()
+
+
+def send_kernel(pick, group, out, here, sems):
+    for b in range(ROWS // 256):
+        part = jnp.concatenate(
+            [dot(pick[r, 256 * b : 256 * (b + 1), :], group[...]) for r in range(SLOTS)], axis=1
+        )
+        send_rows(part, here, out, 256 * b, sems.at[b])
+    for b in range(ROWS // 256):
+        send_wait(here, out, 256 * b, sems.at[b])
+
+
+def split3(a):
+    p1 = a.astype(BF16)
+    rest = a - p1.astype(F32)
+    p2 = rest.astype(BF16)
+    return p1, p2, (rest - p2.astype(F32)).astype(BF16)
+
+
+def mix_kernel(group, mix_gate, mix):
+    block = (iota((TOK, 1), 0) // 4) % BLK
+    gates = mix_gate[...].astype(F32)
+    gate_rows = jnp.zeros((TOK, 128), F32)
+    for k in range(BLK):
+        gate_rows = jnp.where(block == k, gates[k : k + 1, :], gate_rows)
+    part = jnp.sum(group[...].astype(F32) * gate_rows, axis=1, keepdims=True)
+    part = jnp.broadcast_to(part, (TOK, 128))
+    a, b = iota((TOK, TOK), 0), iota((TOK, TOK), 1)
+    mates = ((a // 32 == b // 32) & (a % 4 == b % 4)).astype(F32).astype(BF16)
+    total = sum(dot(mates, p) for p in split3(part))
+    mix[...] = 1.0 / (1.0 + jnp.exp(-total))
+
+
+def weigh_kernel(tp, info, mix, combine):
+    facts = info[...]
     id0, id1 = facts[:, 0:1], facts[:, 1:2]
     w0, w1 = facts[:, 2:3] + facts[:, 3:4], facts[:, 4:5] + facts[:, 5:6]
-    chip, r = col // MSG, col % 4
+    token, place = iota((TOK, ROWS), 0), iota((TOK, ROWS), 1)
+    same, chip, t, i = parts_of(token, place)
     expert = (chip // 2).astype(F32)
     is0, is1 = id0 == expert, id1 == expert
     chosen = jnp.where(is0 | is1, 1.0, 0.0)
-    ra, rb = iota((n, n), 0), iota((n, n), 1)
-    before = ((rb // 4) % 2 == 0) & (rb // 8 * 4 + rb % 4 < ra // 8 * 4 + ra % 4)
-    earlier = dot(before.astype(F32).astype(BF16), chosen.astype(BF16))
-    same_half = (row // 4) % 2 == (col // 4) % 2
-    slot = same_half & (r < 2) & (chosen > 0.5) & (earlier == r.astype(F32))
-    mine = same_half & (r >= 2) & (row // 8 == tp[0]) & (row % 4 == r - 2 + 2 * (chip % 2))
-    pick[...] = jnp.where(slot | mine, 1.0, 0.0).T.astype(BF16)
-    weight[...] = jnp.where(slot, jnp.where(is0, w0, w1), 0.0)
-    mine_out[...] = jnp.where(mine, 1.0, 0.0)
-    for group in copies[1:]:
-        for c in group:
-            c.wait()
-
-
-def send_kernel(pick, group, out, here, sems):
-    for b in range(ROWS // 256):
-        part = dot(pick[256 * b : 256 * (b + 1), :], group[...])
-        send_rows(part, here, out, 256 * b, sems.at[b])
-    for b in range(ROWS // 256):
-        send_wait(here, out, 256 * b, sems.at[b])
-
-
-def mix_kernel(group, mix_gate, mix):
-    n = TP * 8
-    first_half = (iota((n, 1), 0) // 4) % 2 == 0
-    gates = mix_gate[...].astype(F32)
-    gate_rows = jnp.where(first_half, gates[0:1, :], gates[1:2, :])
-    part = jnp.sum(group[...].astype(F32) * gate_rows, axis=1, keepdims=True)
-    part = jnp.broadcast_to(part, (n, 128))
-    other = jnp.where(first_half, pltpu.roll(part, n - 4, 0), pltpu.roll(part, 4, 0))
-    mix[...] = 1.0 / (1.0 + jnp.exp(-(part + other)))
-
-
-def weigh_kernel(mix, weight, mine, combine):
-    total = weight[...] + mine[...] * mix[:, 0:1]
-    high = total.astype(BF16)
-    combine[0] = high
-    combine[1] = (total - high.astype(F32)).astype(BF16)
+    earlier = dot(before(iota((TOK, TOK), 1), iota((TOK, TOK), 0)), chosen.astype(BF16))
+    weight = jnp.where(same & (chosen > 0.5), jnp.where(is0, w0, w1), 0.0)
+    mine = is_mine(tp[0], same, chip, t, i)
+    for r in range(SLOTS):
+        if r < 2:
+            total = jnp.where(earlier == float(r), weight, 0.0)
+        else:
+            total = jnp.where(mine, mix[:, 0:1], 0.0)
+        high = total.astype(BF16)
+        combine[0, r] = high
+        combine[1, r] = (total - high.astype(F32)).astype(BF16)
 
 
 def rows_copy(here, out, first, sem):
@@ -332,7 +381,7 @@
     rows_copy(here, out, first, sem).wait()
 
 
-def expert_kernel(x, own_hbm, sib, dense_y, dense_yc, out, own, here, sems):
+def expert_kernel(x, own_hbm, sib, dense_own, dense_sib, out, own, here, sems):
     step = PACK // 8
     copies = [
         pltpu.make_async_copy(
@@ -344,9 +393,8 @@
         c.start()
 
     def place(dim):
-        k = iota((256, 256), dim)
-        i = k % 64
-        return (i // 2) * MSG + i % 2 + 2 * (k // 64 % 2) + 4 * (k // 128)
+        n = iota((256, 256), dim)
+        return n % 32 * BLK + n // 32
 
     order = (iota((256, 256), 1) == place(0)).astype(F32).astype(BF16)
     back = (iota((256, 256), 0) == place(1)).astype(F32).astype(BF16)
@@ -354,8 +402,11 @@
     xs, xd = [], []
     for b in range(blocks):
         y = dot(order, x[256 * b : 256 * (b + 1), :]).astype(BF16)
-        xs.append(jnp.concatenate([y[0:64], y[128:192]], axis=1))
-        xd.append(jnp.concatenate([y[64:128], y[192:256]], axis=1))
+        for r in range(SLOTS):
+            row = jnp.concatenate(
+                [y[32 * k : 32 * (k + 1), 128 * r : 128 * (r + 1)] for k in range(BLK)], axis=1
+            )
+            (xs if r < 2 else xd).append(row)
     xs, xd = jnp.concatenate(xs, axis=0), jnp.concatenate(xd, axis=0)
 
     def hidden(g, u):
@@ -373,7 +424,11 @@
         total = part if total is None else total + part
 
     def stack(base):
-        parts = [ref[base : base + 32, :] for ref in (dense_y, dense_yc)]
+        parts = [
+            ref[DENSE_ROWS * n + base : DENSE_ROWS * n + base + 32, :]
+            for ref in (dense_own, dense_sib)
+            for n in range(3)
+        ]
         for w in (own, sib):
             first = EXPERT_ROWS + base
             parts.append(
@@ -388,16 +443,25 @@
     dense = dot(h_dense, stack(64)).astype(BF16)
     total = total.astype(BF16)
     for b in range(blocks):
-        part = jnp.concatenate([total[64 * b : 64 * (b + 1)], dense[64 * b : 64 * (b + 1)]], axis=0)
-        part = jnp.concatenate([part[:, :HALF], part[:, HALF:]], axis=0)
+        rows = [total[64 * b : 64 * b + 32], total[64 * b + 32 : 64 * b + 64], dense[32 * b : 32 * b + 32]]
+        part = jnp.concatenate(
+            [
+                jnp.concatenate([a[:, 128 * k : 128 * (k + 1)] for a in rows], axis=1)
+                for k in range(BLK)
+            ],
+            axis=0,
+        )
         send_rows(dot(back, part), here, out, 256 * b, sems.at[8 + b])
     for b in range(blocks):
         send_wait(here, out, 256 * b, sems.at[8 + b])
 
 
 def combine_kernel(combine, returned, out):
-    got = returned[...]
-    total = dot(combine[0], got) + dot(combine[1], got)
+    total = None
+    for r in range(SLOTS):
+        got = returned[:, 128 * r : 128 * (r + 1)]
+        part = dot(combine[0, r], got) + dot(combine[1, r], got)
+        total = part if total is None else total + part
     out[...] = total.astype(BF16)
 
 
@@ -405,7 +469,7 @@
     total = parts[0].astype(F32)
     for t in range(1, TP):
         total = total + parts[t].astype(F32)
-    total = jnp.concatenate([total[0:4, :], total[4:8, :]], axis=1)
+    total = jnp.concatenate([total[4 * k : 4 * (k + 1), :] for k in range(BLK)], axis=1)
     out[...] = (residual[...].astype(F32) + total).astype(BF16)
 
 
@@ -479,6 +543,10 @@
     w_own = a2a(packed, "x")
     w_sib = swap(w_own, "c")
     dense_y = swap(dense_own, "y")
+    dense_z = swap(dense_own, "z")
+    both = [(n, n ^ 9) for n in range(CHIPS)]
+    dense_v = lax.ppermute(dense_own, ("z", "y"), both)
+    dense_three = call(join_kernel, shape(3 * DENSE_ROWS, D), [VMEM] * 3)(dense_y, dense_z, dense_v)
     expert_own = call(
         expert_pack_kernel,
         pltpu.HBM((PACK, 256), BF16),
@@ -492,18 +560,17 @@
         in_hbm(dense_own),
     )
     expert_sib = swap(expert_own, "c")
-    dense_yc = swap(dense_y, "c")
+    dense_three_sib = swap(dense_three, "c")
     attn_in = call(norm_kernel, shape(OWN, D), [VMEM] * 2)(tokens, gain_attn.reshape(1, D))
     new_keys, new_values = call(
         kv_kernel, (shape(OWN, 128), shape(OWN, 128)), [VMEM] * 3
     )(attn_in, w_key, w_value)
     cache = pltpu.VMEM((OWN, CACHE, 128), BF16)
-    pick, weight, mine, w_here, keys, values = call(
+    pick, info, w_here, keys, values = call(
         table_kernel,
         (
-            shape(ROWS, TP * 8),
-            shape(TP * 8, ROWS, dtype=F32),
-            shape(TP * 8, ROWS, dtype=F32),
+            shape(SLOTS, ROWS, TOK),
+            shape(TOK, 128, dtype=F32),
             pltpu.VMEM((TP, wlen, 128), BF16),
             cache,
             cache,
@@ -512,7 +579,7 @@
         [pltpu.SemaphoreType.DMA((3, OWN))],
     )(tp, in_hbm(w_own), in_hbm(keys_cache), in_hbm(values_cache))
     residual, sent = call(
-        attend_kernel, (shape(OWN, D), shape(TP, 8, HALF)), [SMEM, SMEM] + [VMEM] * 8
+        attend_kernel, (shape(OWN, D), shape(TP, 32, 128)), [SMEM, SMEM] + [VMEM] * 8
     )(
         core,
         lengths,
@@ -526,46 +593,42 @@
         gain_ffn.reshape(1, D),
     )
     group = a2a(sent, "x")
-    group = group.reshape(TP * 8, HALF)
+    group = group.reshape(TOK, 128)
     rows = call(
         send_kernel,
-        pltpu.HBM((ROWS, HALF), BF16),
+        pltpu.HBM((ROWS, WIDE), BF16),
         [VMEM] * 2,
-        [pltpu.VMEM((ROWS, HALF), BF16), pltpu.SemaphoreType.DMA((2,))],
+        [pltpu.VMEM((ROWS, WIDE), BF16), pltpu.SemaphoreType.DMA((2,))],
         outs=HBM,
     )(pick, group)
-    mix = call(mix_kernel, shape(TP * 8, 128, dtype=F32), [VMEM] * 2)(
-        group, mix_gate.reshape(2, HALF)
-    )
-    combine = call(weigh_kernel, shape(2, TP * 8, ROWS), [VMEM] * 3)(
-        mix, weight, mine
-    )
-    received = a2a(rows.reshape(CHIPS, MSG, HALF), ("z", "y"))
-    sources = (expert_sib, dense_y, dense_yc)
+    mix = call(mix_kernel, shape(TOK, 128, dtype=F32), [VMEM] * 2)(
+        group, mix_gate.reshape(BLK, 128)
+    )
+    combine = call(
+        weigh_kernel, shape(2, SLOTS, TOK, ROWS), [SMEM, VMEM, VMEM], limit=8
+    )(tp, info, mix)
+    received = a2a(rows.reshape(CHIPS, MSG, WIDE), ("z", "y"))
+    sources = (expert_sib,)
     fetched = call(
-        fetch_kernel,
-        tuple(pltpu.VMEM(a.shape, BF16) for a in sources),
-        [HBM] * 3,
-        [pltpu.SemaphoreType.DMA((3, 4))],
-        8,
+        fetch_kernel, (pltpu.VMEM((PACK, 256), BF16),), [HBM], [pltpu.SemaphoreType.DMA((1, 4))]
     )(*(in_hbm(a) for a in sources))
     outs = call(
         expert_kernel,
-        pltpu.HBM((ROWS, HALF), BF16),
+        pltpu.HBM((ROWS, WIDE), BF16),
         [VMEM, HBM] + [VMEM] * 3,
         [
             pltpu.VMEM((PACK, 256), BF16),
-            pltpu.VMEM((ROWS, HALF), BF16),
+            pltpu.VMEM((ROWS, WIDE), BF16),
             pltpu.SemaphoreType.DMA((10,)),
         ],
         16,
         HBM,
-    )(received.reshape(ROWS, HALF), in_hbm(expert_own), *(in_vmem(a) for a in fetched))
-    returned = a2a(outs.reshape(CHIPS, MSG, HALF), ("z", "y"))
-    partial = call(combine_kernel, shape(TP * 8, HALF), [VMEM] * 2)(
-        combine, returned.reshape(ROWS, HALF)
-    )
-    parts = a2a(partial.reshape(TP, 8, HALF), "x")
+    )(received.reshape(ROWS, WIDE), in_hbm(expert_own), *(in_vmem(a) for a in (*fetched, dense_three, dense_three_sib)))
+    returned = a2a(outs.reshape(CHIPS, MSG, WIDE), ("z", "y"))
+    partial = call(combine_kernel, shape(TOK, 128), [VMEM] * 2)(
+        combine, returned.reshape(ROWS, WIDE)
+    )
+    parts = a2a(partial.reshape(TP, 32, 128), "x")
     layer_out = call(finish_kernel, shape(OWN, D), [VMEM] * 2)(residual, parts)
     return (layer_out, new_keys, new_values)
 

time: 126 us -> 117 us (0.929)
  blocking collectives: 27.4 us -> 19.5 us
  waiting for transfers between devices: 38 us -> 32.6 us
  starting transfers between devices: 41.2 us -> 44.5 us
    ppermute x4 -> x5, waiting for transfers between devices: 14.1 us -> 0.51 us  [swap(): lax.ppermute(array, axis, [(i, i ^ 1) for i in range(lax.axis_size(axis))])]
    all_to_all x3 -> x4, waiting for transfers between devices: 23.9 us -> 32.1 us  [a2a(): return lax.all_to_all(array, axis, split_axis=0, concat_axis=0, tiled=True)]
    all_to_all x2 -> x1, blocking collectives: 27.4 us -> 19.5 us  [a2a(): return lax.all_to_all(array, axis, split_axis=0, concat_axis=0, tiled=True)]
    ppermute x4 -> x5, starting transfers between devices: 8.59 us -> 12.9 us  [swap(): lax.ppermute(array, axis, [(i, i ^ 1) for i in range(lax.axis_size(axis))])]
    all_to_all x3 -> x4, starting transfers between devices: 32.6 us -> 28.7 us  [a2a(): return lax.all_to_all(array, axis, split_axis=0, concat_axis=0, tiled=True)]
    ppermute x0 -> x1, starting transfers between devices: none -> 2.93 us  [body(): dense_v = lax.ppermute(dense_own, ('z', 'y'), both)]
    pallas_call x8 -> x9, Pallas kernels: 11.3 us -> 12.5 us  [the longest x1 3.58 us: body(): call(expert_kernel, pltpu.HBM((ROWS, WIDE), BF16), [VMEM, HBM] + [VMEM] *...]
  transfers between devices with their start and end apart: 7 -> 10, of which waited for: 4 -> 4; matrix products, arithmetic and copies ran while one was open for 0% -> 0% of each run, Pallas kernels for 8% -> 10%
where the time goes in v3:
time: 117 us; the launch traced here: 116 us
  starting transfers between devices  44.5 us (38%)
  waiting for transfers between devices  32.6 us (28%)
  blocking collectives  19.5 us (17%)
  Pallas kernels  18.5 us (16%)
    all_to_all x4, waiting for transfers between devices, a2a(): return lax.all_to_all(array, axis, split_axis=0, concat_axis=0, tiled=True)  32.1 us
    all_to_all x4, starting transfers between devices, a2a(): return lax.all_to_all(array, axis, split_axis=0, concat_axis=0, tiled=True)  28.7 us
    all_to_all x1, blocking collectives, a2a(): return lax.all_to_all(array, axis, split_axis=0, concat_axis=0, tiled=True)  19.5 us
    ppermute x5, starting transfers between devices, swap(): lax.ppermute(array, axis, [(i, i ^ 1) for i in range(lax.axis_size(axis))])  12.9 us
    pallas_call x1, Pallas kernels, body(): call(expert_kernel, pltpu.HBM((ROWS, WIDE), BF16), [VMEM, HBM] + [VMEM] *...  3.58 us
    ppermute x1, starting transfers between devices, body(): dense_v = lax.ppermute(dense_own, ('z', 'y'), both)  2.93 us
    pallas_call x1, Pallas kernels, body(): call(attend_kernel, (shape(OWN, D), shape(TP, 32, 128)), [SMEM, SMEM] + [...  2.8 us
    pallas_call x1, Pallas kernels, body(): call(expert_pack_kernel, pltpu.HBM((PACK, 256), BF16), [HBM] * 4, [pltpu....  2.43 us
  transfers between devices with their start and end apart: 10, of which 4 were waited for; matrix products, arithmetic and copies ran while one was open for 0% of the time, Pallas kernels for 10%

profile of v3, /device:TPU:8, one launch (start us, length us, event | category | flops | bytes accessed | tf_op | source)
XLA Modules:
  0.0 116.1 jit_solution(4911960795343863455)
XLA Ops:
  0.6 2.2 %shard_map.212 = (bf16[4,1032,128]{2,1,0:T(8,128)(2,1)}, bf16[96,1024]{1,0:T(8,128)(2,1)}) custom-call(s32[1]{0:T(128)} %bitcast.core, bf16[1024,128]{1,0:T(8,128)(2,1)} %wq.1, bf16[128,1024]{1,0:T(8,128)(2,1)} %wo.1, s32[2,4]{1,0:T(2,128)} %bitcast.26, f32[2,4]{1,0:T(2,128)} %bitcast.27, bf16[32,1024]{1,0:T(8,128)(2,1)} %gate.1, bf16[32,1024]{1,0:T(8,128)(2,1)} %up.1, ...), custom_call_target="tpu_custom_call" | custom-call | tf_op jit(solution)/shard_map/pallas_call | solution.py:521
  2.8 19.5 %all_to_all.25.own_hbm = bf16[4,1032,128]{2,1,0:T(8,128)(2,1)S(1)} all-to-all(bf16[4,1032,128]{2,1,0:T(8,128)(2,1)} %get-tuple-element.14), channel_id=1, replica_groups=mesh['z'=8,'y'=8,'c'=2,'x'=4] {'x'}, dimensions={0} | all-to-all | bytes 2113536 | tf_op jit(solution)/shard_map/all_to_all | solution.py:489
  22.3 1.9 %collective-permute-start = (bf16[4,1032,128]{2,1,0:T(8,128)(2,1)S(1)}, bf16[4,1032,128]{2,1,0:T(8,128)(2,1)S(1)}, u32[]{:S(2)}, u32[]{:S(2)}) collective-permute-start(bf16[4,1032,128]{2,1,0:T(8,128)(2,1)S(1)} %all_to_all.25.own_hbm), channel_id=1, source_target_pairs={{0,4},{4,0},{1,5},{5,1},{2,6},{6,2},{3,7},{7,3},{8,12},{12,8},{9,1... | collective-permute-start | bytes 3170312 | tf_op jit(solution)/shard_map/ppermute | solution.py:493
  24.2 2.4 %shard_map.218.own_hbm = bf16[3456,256]{1,0:T(8,128)(2,1)} custom-call(bf16[1024,256]{1,0:T(8,128)(2,1)} %bitcast.23, bf16[1024,256]{1,0:T(8,128)(2,1)} %bitcast.24, bf16[256,1024]{1,0:T(8,128)(2,1)} %bitcast.25, bf16[96,1024]{1,0:T(8,128)(2,1)} %get-tuple-element.22.dense), custom_call_target="tpu_custom_call" | custom-call | tf_op jit(solution)/shard_map/pallas_call | solution.py:550
  26.7 2.4 %collective-permute-start.1 = (bf16[3456,256]{1,0:T(8,128)(2,1)}, bf16[3456,256]{1,0:T(8,128)(2,1)}, u32[]{:S(2)}, u32[]{:S(2)}) collective-permute-start(bf16[3456,256]{1,0:T(8,128)(2,1)} %shard_map.218.own_hbm), channel_id=1, source_target_pairs={{0,4},{4,0},{1,5},{5,1},{2,6},{6,2},{3,7},{7,3},{8,12},{12,8},{9,1... | collective-permute-start | bytes 5308424 | tf_op jit(solution)/shard_map/ppermute | solution.py:493
  29.3 2.0 %shard_map.213 = (bf16[3,512,128]{2,1,0:T(8,128)(2,1)S(1)}, f32[128,128]{1,0:T(8,128)S(1)}, bf16[4,1032,128]{2,1,0:T(8,128)(2,1)S(1)}, bf16[4,1024,128]{2,1,0:T(8,128)(2,1)S(1)}, bf16[4,1024,128]{2,1,0:T(8,128)(2,1)S(1)}) custom-call(s32[1]{0:T(128)} %bitcast.1.tp, bf16[4,1032,128]{2,1,0:T(8,128)(2,1)} %copy-done.6, bf16[4,1024,128]{2,1,0:T(8,128)(2,1)} %keys_hbm.1, ...), custom_call_target="tpu_custom_call" | custom-call | tf_op jit(solution)/shard_map/pallas_call | solution.py:569
  31.3 2.8 %shard_map.214 = (bf16[4,1024]{1,0:T(4,128)(2,1)S(1)}, bf16[4,32,128]{2,1,0:T(8,128)(2,1)}) custom-call(s32[1]{0:T(128)} %bitcast.core, s32[4]{0:T(128)S(1)} %copy-done.4, bf16[4,1024]{1,0:T(4,128)(2,1)S(1)} %copy-done.2, bf16[4,1024]{1,0:T(4,128)(2,1)S(1)} %shard_map.211.attn_in, bf16[4,1032,128]{2,1,0:T(8,128)(2,1)S(1)} %get-tuple-element.15.w_own, ...), custom_call_target="tpu_custom_call" | custom-call | tf_op jit(solution)/shard_map/pallas_call | solution.py:581
  34.1 3.3 %all-to-all-start.1 = ((bf16[4,32,128]{2,1,0:T(8,128)(2,1)}), bf16[4,32,128]{2,1,0:T(8,128)(2,1)S(1)}, u32[]{:S(2)}, u32[]{:S(2)}) async-start(bf16[4,32,128]{2,1,0:T(8,128)(2,1)} %get-tuple-element.20), calls=%async_computation.1 | async-start | bytes 65536 | tf_op jit(solution)/shard_map/all_to_all | solution.py:489
  37.3 2.6 %collective-permute-start.2 = (bf16[96,1024]{1,0:T(8,128)(2,1)S(1)}, bf16[96,1024]{1,0:T(8,128)(2,1)S(1)}, u32[]{:S(2)}, u32[]{:S(2)}) collective-permute-start(bf16[96,1024]{1,0:T(8,128)(2,1)S(1)} %copy-done.7), channel_id=1, source_target_pairs={{0,8},{8,0},{16,24},{24,16},{32,40},{40,32},{48,56},{56,48},{1,9},... | collective-permute-start | bytes 589832 | tf_op jit(solution)/shard_map/ppermute | solution.py:493
  40.0 4.0 %collective-permute-start.3 = (bf16[96,1024]{1,0:T(8,128)(2,1)S(1)}, bf16[96,1024]{1,0:T(8,128)(2,1)S(1)}, u32[]{:S(2)}, u32[]{:S(2)}) collective-permute-start(bf16[96,1024]{1,0:T(8,128)(2,1)S(1)} %copy-done.7), channel_id=1, source_target_pairs={{0,64},{64,0},{128,192},{192,128},{256,320},{320,256},{384,448},{4... | collective-permute-start | bytes 589832 | tf_op jit(solution)/shard_map/ppermute | solution.py:493
  44.0 2.9 %collective-permute-start.4 = (bf16[96,1024]{1,0:T(8,128)(2,1)S(1)}, bf16[96,1024]{1,0:T(8,128)(2,1)S(1)}, u32[]{:S(2)}, u32[]{:S(2)}) collective-permute-start(bf16[96,1024]{1,0:T(8,128)(2,1)S(1)} %copy-done.7), channel_id=1, source_target_pairs={{0,72},{8,64},{16,88},{24,80},{32,104},{40,96},{48,120},{56,112},{... | collective-permute-start | bytes 589832 | tf_op jit(solution)/shard_map/ppermute | solution.py:548
  47.0 1.0 shard_map.217
  47.9 16.2 %all-to-all-start.2 = ((bf16[64,8,384]{2,1,0:T(8,128)(2,1)}), bf16[64,8,384]{2,1,0:T(8,128)(2,1)S(1)}, u32[]{:S(2)}, u32[]{:S(2)}) async-start(bf16[64,8,384]{2,1,0:T(8,128)(2,1)} %bitcast.21), calls=%async_computation.2 | async-start | bytes 786432 | tf_op jit(solution)/shard_map/all_to_all | solution.py:489
  64.3 1.9 %collective-permute-start.5 = (bf16[288,1024]{1,0:T(8,128)(2,1)S(1)}, bf16[288,1024]{1,0:T(8,128)(2,1)S(1)}, u32[]{:S(2)}, u32[]{:S(2)}) collective-permute-start(bf16[288,1024]{1,0:T(8,128)(2,1)S(1)} %shard_map.220.dense_own), channel_id=1, source_target_pairs={{0,4},{4,0},{1,5},{5,1},{2,6},{6,2},{3,7},{7,3},{8,12},{12,8},{9,1... | collective-permute-start | bytes 1769480 | tf_op jit(solution)/shard_map/ppermute | solution.py:493
  66.2 1.4 %shard_map.219.sib = bf16[3456,256]{1,0:T(8,128)(2,1)S(1)} custom-call(bf16[3456,256]{1,0:T(8,128)(2,1)} %collective-permute-done.1.refs_0_), custom_call_target="tpu_custom_call" | custom-call | tf_op jit(solution)/shard_map/pallas_call | solution.py:612
  68.2 12.3 %all-to-all-done.2 = bf16[64,8,384]{2,1,0:T(8,128)(2,1)S(1)} async-done(((bf16[64,8,384]{2,1,0:T(8,128)(2,1)}), bf16[64,8,384]{2,1,0:T(8,128)(2,1)S(1)}, u32[]{:S(2)}, u32[]{:S(2)}) %all-to-all-start.2) | async-done | bytes 393248 | tf_op jit(solution)/shard_map/all_to_all | solution.py:489
  80.4 3.6 %shard_map.221 = bf16[512,384]{1,0:T(8,128)(2,1)} custom-call(bf16[512,384]{1,0:T(8,128)(2,1)S(1)} %bitcast.16, bf16[3456,256]{1,0:T(8,128)(2,1)} %shard_map.218.own_hbm, bf16[3456,256]{1,0:T(8,128)(2,1)S(1)} %shard_map.219.sib, bf16[288,1024]{1,0:T(8,128)(2,1)S(1)} %shard_map.220.dense_own, bf16[288,1024]{1,0:T(8,128)(2,1)S(1)} %collective-permute-done.5.dense_sib), custom_call_target="tpu_custom_call" | custom-call | tf_op jit(solution)/shard_map/pallas_call | solution.py:615
  84.0 5.0 %all-to-all-start.3 = ((bf16[64,8,384]{2,1,0:T(8,128)(2,1)}), bf16[64,8,384]{2,1,0:T(8,128)(2,1)S(1)}, u32[]{:S(2)}, u32[]{:S(2)}) async-start(bf16[64,8,384]{2,1,0:T(8,128)(2,1)} %bitcast.22), calls=%async_computation.3 | async-start | bytes 786432 | tf_op jit(solution)/shard_map/all_to_all | solution.py:489
  89.8 15.1 %all-to-all-done.3 = bf16[64,8,384]{2,1,0:T(8,128)(2,1)S(1)} async-done(((bf16[64,8,384]{2,1,0:T(8,128)(2,1)}), bf16[64,8,384]{2,1,0:T(8,128)(2,1)S(1)}, u32[]{:S(2)}, u32[]{:S(2)}) %all-to-all-start.3) | async-done | bytes 393248 | tf_op jit(solution)/shard_map/all_to_all | solution.py:489
  104.9 1.0 shard_map.222
  105.9 4.2 %all-to-all-start.4 = ((bf16[4,32,128]{2,1,0:T(8,128)(2,1)}), bf16[4,32,128]{2,1,0:T(8,128)(2,1)S(1)}, u32[]{:S(2)}, u32[]{:S(2)}) async-start(bf16[4,32,128]{2,1,0:T(8,128)(2,1)} %bitcast.14), calls=%async_computation.4 | async-start | bytes 65536 | tf_op jit(solution)/shard_map/all_to_all | solution.py:489
  110.1 0.8 shard_map.224
  110.8 4.7 %all-to-all-done.4.parts = bf16[4,32,128]{2,1,0:T(8,128)(2,1)S(1)} async-done(((bf16[4,32,128]{2,1,0:T(8,128)(2,1)}), bf16[4,32,128]{2,1,0:T(8,128)(2,1)S(1)}, u32[]{:S(2)}, u32[]{:S(2)}) %all-to-all-start.4) | async-done | bytes 32800 | tf_op jit(solution)/shard_map/all_to_all | solution.py:489
  115.5 0.6 shard_map.223
  (33 shorter events, 1.4 us)
Async XLA Ops:
  22.3 4.4 %copy-start.6 = (bf16[4,1032,128]{2,1,0:T(8,128)(2,1)}, bf16[4,1032,128]{2,1,0:T(8,128)(2,1)S(1)}, u32[]{:S(2)}) copy-start(bf16[4,1032,128]{2,1,0:T(8,128)(2,1)S(1)} %all_to_all.25.own_hbm) | copy-start | bytes 3170308
  22.3 8.9 %collective-permute-start = (bf16[4,1032,128]{2,1,0:T(8,128)(2,1)S(1)}, bf16[4,1032,128]{2,1,0:T(8,128)(2,1)S(1)}, u32[]{:S(2)}, u32[]{:S(2)}) collective-permute-start(bf16[4,1032,128]{2,1,0:T(8,128)(2,1)S(1)} %all_to_all.25.own_hbm), channel_id=1, source_target_pairs={{0,4},{4,0},{1,5},{5,1},{2,6},{6,2},{3,7},{7,3},{8,12},{12,8},{9,1... | collective-permute-start | bytes 3170312 | tf_op jit(solution)/shard_map/ppermute | solution.py:493
  24.2 4.9 %copy-start.8 = (bf16[1024]{0:T(1024)(128)(2,1)S(1)}, bf16[1024]{0:T(1024)(128)(2,1)}, u32[]{:S(2)}) copy-start(bf16[1024]{0:T(1024)(128)(2,1)} %param.21) | copy-start | bytes 6148
  24.2 4.9 %copy-start.9 = (bf16[1024]{0:T(1024)(128)(2,1)S(1)}, bf16[1024]{0:T(1024)(128)(2,1)}, u32[]{:S(2)}) copy-start(bf16[1024]{0:T(1024)(128)(2,1)} %param.22) | copy-start | bytes 6148
  24.2 4.9 %copy-start.2 = (bf16[4,1024]{1,0:T(4,128)(2,1)S(1)}, bf16[4,1024]{1,0:T(4,128)(2,1)}, u32[]{:S(2)}) copy-start(bf16[4,1024]{1,0:T(4,128)(2,1)} %tokens.3) | copy-start | bytes 24580
  26.7 39.5 %collective-permute-start.1 = (bf16[3456,256]{1,0:T(8,128)(2,1)}, bf16[3456,256]{1,0:T(8,128)(2,1)}, u32[]{:S(2)}, u32[]{:S(2)}) collective-permute-start(bf16[3456,256]{1,0:T(8,128)(2,1)} %shard_map.218.own_hbm), channel_id=1, source_target_pairs={{0,4},{4,0},{1,5},{5,1},{2,6},{6,2},{3,7},{7,3},{8,12},{12,8},{9,1... | collective-permute-start | bytes 5308424 | tf_op jit(solution)/shard_map/ppermute | solution.py:493
  29.3 2.0 %copy-start.4 = (s32[4]{0:T(128)S(1)}, s32[4]{0:T(128)}, u32[]{:S(2)}) copy-start(s32[4]{0:T(128)} %lengths.1) | copy-start | bytes 52
  29.3 2.0 %copy-start.5 = (f32[8]{0:T(128)S(1)}, f32[8]{0:T(128)}, u32[]{:S(2)}) copy-start(f32[8]{0:T(128)} %param.27) | copy-start | bytes 100
  31.3 6.1 %copy-start.7 = (bf16[96,1024]{1,0:T(8,128)(2,1)S(1)}, bf16[96,1024]{1,0:T(8,128)(2,1)}, u32[]{:S(2)}) copy-start(bf16[96,1024]{1,0:T(8,128)(2,1)} %get-tuple-element.22.dense) | copy-start | bytes 589828
  34.1 12.9 %all-to-all-start.1 = ((bf16[4,32,128]{2,1,0:T(8,128)(2,1)}), bf16[4,32,128]{2,1,0:T(8,128)(2,1)S(1)}, u32[]{:S(2)}, u32[]{:S(2)}) async-start(bf16[4,32,128]{2,1,0:T(8,128)(2,1)} %get-tuple-element.20), calls=%async_computation.1 | async-start | bytes 65536 | tf_op jit(solution)/shard_map/all_to_all | solution.py:489
  37.3 26.8 %collective-permute-start.2 = (bf16[96,1024]{1,0:T(8,128)(2,1)S(1)}, bf16[96,1024]{1,0:T(8,128)(2,1)S(1)}, u32[]{:S(2)}, u32[]{:S(2)}) collective-permute-start(bf16[96,1024]{1,0:T(8,128)(2,1)S(1)} %copy-done.7), channel_id=1, source_target_pairs={{0,8},{8,0},{16,24},{24,16},{32,40},{40,32},{48,56},{56,48},{1,9},... | collective-permute-start | bytes 589832 | tf_op jit(solution)/shard_map/ppermute | solution.py:493
  40.0 24.2 %collective-permute-start.3 = (bf16[96,1024]{1,0:T(8,128)(2,1)S(1)}, bf16[96,1024]{1,0:T(8,128)(2,1)S(1)}, u32[]{:S(2)}, u32[]{:S(2)}) collective-permute-start(bf16[96,1024]{1,0:T(8,128)(2,1)S(1)} %copy-done.7), channel_id=1, source_target_pairs={{0,64},{64,0},{128,192},{192,128},{256,320},{320,256},{384,448},{4... | collective-permute-start | bytes 589832 | tf_op jit(solution)/shard_map/ppermute | solution.py:493
  44.0 20.2 %collective-permute-start.4 = (bf16[96,1024]{1,0:T(8,128)(2,1)S(1)}, bf16[96,1024]{1,0:T(8,128)(2,1)S(1)}, u32[]{:S(2)}, u32[]{:S(2)}) collective-permute-start(bf16[96,1024]{1,0:T(8,128)(2,1)S(1)} %copy-done.7), channel_id=1, source_target_pairs={{0,72},{8,64},{16,88},{24,80},{32,104},{40,96},{48,120},{56,112},{... | collective-permute-start | bytes 589832 | tf_op jit(solution)/shard_map/ppermute | solution.py:548
  47.9 32.5 %all-to-all-start.2 = ((bf16[64,8,384]{2,1,0:T(8,128)(2,1)}), bf16[64,8,384]{2,1,0:T(8,128)(2,1)S(1)}, u32[]{:S(2)}, u32[]{:S(2)}) async-start(bf16[64,8,384]{2,1,0:T(8,128)(2,1)} %bitcast.21), calls=%async_computation.2 | async-start | bytes 786432 | tf_op jit(solution)/shard_map/all_to_all | solution.py:489
  64.3 3.9 %collective-permute-start.5 = (bf16[288,1024]{1,0:T(8,128)(2,1)S(1)}, bf16[288,1024]{1,0:T(8,128)(2,1)S(1)}, u32[]{:S(2)}, u32[]{:S(2)}) collective-permute-start(bf16[288,1024]{1,0:T(8,128)(2,1)S(1)} %shard_map.220.dense_own), channel_id=1, source_target_pairs={{0,4},{4,0},{1,5},{5,1},{2,6},{6,2},{3,7},{7,3},{8,12},{12,8},{9,1... | collective-permute-start | bytes 1769480 | tf_op jit(solution)/shard_map/ppermute | solution.py:493
  80.4 8.6 %copy-start.3 = (bf16[1024]{0:T(1024)(128)(2,1)S(1)}, bf16[1024]{0:T(1024)(128)(2,1)}, u32[]{:S(2)}) copy-start(bf16[1024]{0:T(1024)(128)(2,1)} %param.34) | copy-start | bytes 6148
  84.0 20.9 %all-to-all-start.3 = ((bf16[64,8,384]{2,1,0:T(8,128)(2,1)}), bf16[64,8,384]{2,1,0:T(8,128)(2,1)S(1)}, u32[]{:S(2)}, u32[]{:S(2)}) async-start(bf16[64,8,384]{2,1,0:T(8,128)(2,1)} %bitcast.22), calls=%async_computation.3 | async-start | bytes 786432 | tf_op jit(solution)/shard_map/all_to_all | solution.py:489
  89.3 20.8 %copy-start = (bf16[1024,128]{1,0:T(8,128)(2,1)S(1)}, bf16[1024,128]{1,0:T(8,128)(2,1)}, u32[]{:S(2)}) copy-start(bf16[1024,128]{1,0:T(8,128)(2,1)} %wk.1) | copy-start | bytes 786436
  89.3 20.7 %copy-start.1 = (bf16[1024,128]{1,0:T(8,128)(2,1)S(1)}, bf16[1024,128]{1,0:T(8,128)(2,1)}, u32[]{:S(2)}) copy-start(bf16[1024,128]{1,0:T(8,128)(2,1)} %wv.1) | copy-start | bytes 786436
  105.9 9.6 %all-to-all-start.4 = ((bf16[4,32,128]{2,1,0:T(8,128)(2,1)}), bf16[4,32,128]{2,1,0:T(8,128)(2,1)S(1)}, u32[]{:S(2)}, u32[]{:S(2)}) async-start(bf16[4,32,128]{2,1,0:T(8,128)(2,1)} %bitcast.14), calls=%async_computation.4 | async-start | bytes 65536 | tf_op jit(solution)/shard_map/all_to_all | solution.py:489

commit v4 on v3

--- a/solution.py
+++ b/solution.py
@@ -382,12 +382,11 @@
 
 
 def expert_kernel(x, own_hbm, sib, dense_own, dense_sib, out, own, here, sems):
-    step = PACK // 8
+    edges = [EXPERT_ROWS, PACK], [0, HALF], [HALF, D], [D, D + HALF], [D + HALF, 2 * D]
+    edges = (*edges, [2 * D, 2 * D + HALF], [2 * D + HALF, EXPERT_ROWS])
     copies = [
-        pltpu.make_async_copy(
-            own_hbm.at[k * step : (k + 1) * step, :], own.at[k * step : (k + 1) * step, :], sems.at[k]
-        )
-        for k in range(8)
+        pltpu.make_async_copy(own_hbm.at[lo:hi, :], own.at[lo:hi, :], sems.at[k])
+        for k, (lo, hi) in enumerate(edges)
     ]
     for c in copies:
         c.start()
@@ -412,16 +411,10 @@
     def hidden(g, u):
         return (g / (1.0 + jnp.exp(-g)) * u).astype(BF16)
 
-    total = None
-    for w in (sib, own):
-        if w is own:
-            for c in copies:
-                c.wait()
-        h = hidden(dot(xs, w[0:D, :]), dot(xs, w[D : 2 * D, :]))
-        part = jnp.concatenate(
+    def down(h, w):
+        return jnp.concatenate(
             [dot(h, w[2 * D + 256 * j : 2 * D + 256 * (j + 1), :]) for j in range(4)], axis=1
         )
-        total = part if total is None else total + part
 
     def stack(base):
         parts = [
@@ -439,8 +432,19 @@
             )
         return jnp.concatenate(parts, axis=0)
 
+    total = down(hidden(dot(xs, sib[0:D, :]), dot(xs, sib[D : 2 * D, :])), sib)
+    copies[0].wait()
     h_dense = hidden(dot_t(xd, stack(0)), dot_t(xd, stack(32)))
     dense = dot(h_dense, stack(64)).astype(BF16)
+    for c in copies[1:3]:
+        c.wait()
+    g = dot(xs, own[0:D, :])
+    for c in copies[3:5]:
+        c.wait()
+    h = hidden(g, dot(xs, own[D : 2 * D, :]))
+    for c in copies[5:7]:
+        c.wait()
+    total = total + down(h, own)
     total = total.astype(BF16)
     for b in range(blocks):
         rows = [total[64 * b : 64 * b + 32], total[64 * b + 32 : 64 * b + 64], dense[32 * b : 32 * b + 32]]

time: 117 us -> 117 us (level)
  no operation moved by 1% of the time
where the time goes in v4:
time: 117 us; the launch traced here: 116 us
  starting transfers between devices  44.5 us (38%)
  waiting for transfers between devices  32.6 us (28%)
  blocking collectives  19.5 us (17%)
  Pallas kernels  18.4 us (16%)
    all_to_all x4, waiting for transfers between devices, a2a(): return lax.all_to_all(array, axis, split_axis=0, concat_axis=0, tiled=True)  32.1 us
    all_to_all x4, starting transfers between devices, a2a(): return lax.all_to_all(array, axis, split_axis=0, concat_axis=0, tiled=True)  28.7 us
    all_to_all x1, blocking collectives, a2a(): return lax.all_to_all(array, axis, split_axis=0, concat_axis=0, tiled=True)  19.5 us
    ppermute x5, starting transfers between devices, swap(): lax.ppermute(array, axis, [(i, i ^ 1) for i in range(lax.axis_size(axis))])  12.9 us
    pallas_call x1, Pallas kernels, body(): call(expert_kernel, pltpu.HBM((ROWS, WIDE), BF16), [VMEM, HBM] + [VMEM] *...  3.42 us
    ppermute x1, starting transfers between devices, body(): dense_v = lax.ppermute(dense_own, ('z', 'y'), both)  2.93 us
    pallas_call x1, Pallas kernels, body(): call(attend_kernel, (shape(OWN, D), shape(TP, 32, 128)), [SMEM, SMEM] + [...  2.8 us
    pallas_call x1, Pallas kernels, body(): call(expert_pack_kernel, pltpu.HBM((PACK, 256), BF16), [HBM] * 4, [pltpu....  2.43 us
  transfers between devices with their start and end apart: 10, of which 4 were waited for; matrix products, arithmetic and copies ran while one was open for 0% of the time, Pallas kernels for 10%

profile of v4, /device:TPU:8, one launch (start us, length us, event | category | flops | bytes accessed | tf_op | source)
XLA Modules:
  0.0 116.0 jit_solution(11297393394929264115)
XLA Ops:
  0.6 2.2 %shard_map.212 = (bf16[4,1032,128]{2,1,0:T(8,128)(2,1)}, bf16[96,1024]{1,0:T(8,128)(2,1)}) custom-call(s32[1]{0:T(128)} %bitcast.core, bf16[1024,128]{1,0:T(8,128)(2,1)} %wq.1, bf16[128,1024]{1,0:T(8,128)(2,1)} %wo.1, s32[2,4]{1,0:T(2,128)} %bitcast.26, f32[2,4]{1,0:T(2,128)} %bitcast.27, bf16[32,1024]{1,0:T(8,128)(2,1)} %gate.1, bf16[32,1024]{1,0:T(8,128)(2,1)} %up.1, ...), custom_call_target="tpu_custom_call" | custom-call | tf_op jit(solution)/shard_map/pallas_call | solution.py:525
  2.8 19.5 %all_to_all.25.own_hbm = bf16[4,1032,128]{2,1,0:T(8,128)(2,1)S(1)} all-to-all(bf16[4,1032,128]{2,1,0:T(8,128)(2,1)} %get-tuple-element.14), channel_id=1, replica_groups=mesh['z'=8,'y'=8,'c'=2,'x'=4] {'x'}, dimensions={0} | all-to-all | bytes 2113536 | tf_op jit(solution)/shard_map/all_to_all | solution.py:493
  22.3 1.9 %collective-permute-start = (bf16[4,1032,128]{2,1,0:T(8,128)(2,1)S(1)}, bf16[4,1032,128]{2,1,0:T(8,128)(2,1)S(1)}, u32[]{:S(2)}, u32[]{:S(2)}) collective-permute-start(bf16[4,1032,128]{2,1,0:T(8,128)(2,1)S(1)} %all_to_all.25.own_hbm), channel_id=1, source_target_pairs={{0,4},{4,0},{1,5},{5,1},{2,6},{6,2},{3,7},{7,3},{8,12},{12,8},{9,1... | collective-permute-start | bytes 3170312 | tf_op jit(solution)/shard_map/ppermute | solution.py:497
  24.2 2.4 %shard_map.218.own_hbm = bf16[3456,256]{1,0:T(8,128)(2,1)} custom-call(bf16[1024,256]{1,0:T(8,128)(2,1)} %bitcast.23, bf16[1024,256]{1,0:T(8,128)(2,1)} %bitcast.24, bf16[256,1024]{1,0:T(8,128)(2,1)} %bitcast.25, bf16[96,1024]{1,0:T(8,128)(2,1)} %get-tuple-element.22.dense), custom_call_target="tpu_custom_call" | custom-call | tf_op jit(solution)/shard_map/pallas_call | solution.py:554
  26.7 2.4 %collective-permute-start.1 = (bf16[3456,256]{1,0:T(8,128)(2,1)}, bf16[3456,256]{1,0:T(8,128)(2,1)}, u32[]{:S(2)}, u32[]{:S(2)}) collective-permute-start(bf16[3456,256]{1,0:T(8,128)(2,1)} %shard_map.218.own_hbm), channel_id=1, source_target_pairs={{0,4},{4,0},{1,5},{5,1},{2,6},{6,2},{3,7},{7,3},{8,12},{12,8},{9,1... | collective-permute-start | bytes 5308424 | tf_op jit(solution)/shard_map/ppermute | solution.py:497
  29.3 2.0 %shard_map.213 = (bf16[3,512,128]{2,1,0:T(8,128)(2,1)S(1)}, f32[128,128]{1,0:T(8,128)S(1)}, bf16[4,1032,128]{2,1,0:T(8,128)(2,1)S(1)}, bf16[4,1024,128]{2,1,0:T(8,128)(2,1)S(1)}, bf16[4,1024,128]{2,1,0:T(8,128)(2,1)S(1)}) custom-call(s32[1]{0:T(128)} %bitcast.1.tp, bf16[4,1032,128]{2,1,0:T(8,128)(2,1)} %copy-done.6, bf16[4,1024,128]{2,1,0:T(8,128)(2,1)} %keys_hbm.1, ...), custom_call_target="tpu_custom_call" | custom-call | tf_op jit(solution)/shard_map/pallas_call | solution.py:573
  31.3 2.8 %shard_map.214 = (bf16[4,1024]{1,0:T(4,128)(2,1)S(1)}, bf16[4,32,128]{2,1,0:T(8,128)(2,1)}) custom-call(s32[1]{0:T(128)} %bitcast.core, s32[4]{0:T(128)S(1)} %copy-done.4, bf16[4,1024]{1,0:T(4,128)(2,1)S(1)} %copy-done.2, bf16[4,1024]{1,0:T(4,128)(2,1)S(1)} %shard_map.211.attn_in, bf16[4,1032,128]{2,1,0:T(8,128)(2,1)S(1)} %get-tuple-element.15.w_own, ...), custom_call_target="tpu_custom_call" | custom-call | tf_op jit(solution)/shard_map/pallas_call | solution.py:585
  34.1 3.3 %all-to-all-start.1 = ((bf16[4,32,128]{2,1,0:T(8,128)(2,1)}), bf16[4,32,128]{2,1,0:T(8,128)(2,1)S(1)}, u32[]{:S(2)}, u32[]{:S(2)}) async-start(bf16[4,32,128]{2,1,0:T(8,128)(2,1)} %get-tuple-element.20), calls=%async_computation.1 | async-start | bytes 65536 | tf_op jit(solution)/shard_map/all_to_all | solution.py:493
  37.3 2.6 %collective-permute-start.2 = (bf16[96,1024]{1,0:T(8,128)(2,1)S(1)}, bf16[96,1024]{1,0:T(8,128)(2,1)S(1)}, u32[]{:S(2)}, u32[]{:S(2)}) collective-permute-start(bf16[96,1024]{1,0:T(8,128)(2,1)S(1)} %copy-done.7), channel_id=1, source_target_pairs={{0,8},{8,0},{16,24},{24,16},{32,40},{40,32},{48,56},{56,48},{1,9},... | collective-permute-start | bytes 589832 | tf_op jit(solution)/shard_map/ppermute | solution.py:497
  40.0 4.0 %collective-permute-start.3 = (bf16[96,1024]{1,0:T(8,128)(2,1)S(1)}, bf16[96,1024]{1,0:T(8,128)(2,1)S(1)}, u32[]{:S(2)}, u32[]{:S(2)}) collective-permute-start(bf16[96,1024]{1,0:T(8,128)(2,1)S(1)} %copy-done.7), channel_id=1, source_target_pairs={{0,64},{64,0},{128,192},{192,128},{256,320},{320,256},{384,448},{4... | collective-permute-start | bytes 589832 | tf_op jit(solution)/shard_map/ppermute | solution.py:497
  44.0 2.9 %collective-permute-start.4 = (bf16[96,1024]{1,0:T(8,128)(2,1)S(1)}, bf16[96,1024]{1,0:T(8,128)(2,1)S(1)}, u32[]{:S(2)}, u32[]{:S(2)}) collective-permute-start(bf16[96,1024]{1,0:T(8,128)(2,1)S(1)} %copy-done.7), channel_id=1, source_target_pairs={{0,72},{8,64},{16,88},{24,80},{32,104},{40,96},{48,120},{56,112},{... | collective-permute-start | bytes 589832 | tf_op jit(solution)/shard_map/ppermute | solution.py:552
  47.0 1.0 shard_map.217
  47.9 16.2 %all-to-all-start.2 = ((bf16[64,8,384]{2,1,0:T(8,128)(2,1)}), bf16[64,8,384]{2,1,0:T(8,128)(2,1)S(1)}, u32[]{:S(2)}, u32[]{:S(2)}) async-start(bf16[64,8,384]{2,1,0:T(8,128)(2,1)} %bitcast.21), calls=%async_computation.2 | async-start | bytes 786432 | tf_op jit(solution)/shard_map/all_to_all | solution.py:493
  64.3 1.9 %collective-permute-start.5 = (bf16[288,1024]{1,0:T(8,128)(2,1)S(1)}, bf16[288,1024]{1,0:T(8,128)(2,1)S(1)}, u32[]{:S(2)}, u32[]{:S(2)}) collective-permute-start(bf16[288,1024]{1,0:T(8,128)(2,1)S(1)} %shard_map.220.dense_own), channel_id=1, source_target_pairs={{0,4},{4,0},{1,5},{5,1},{2,6},{6,2},{3,7},{7,3},{8,12},{12,8},{9,1... | collective-permute-start | bytes 1769480 | tf_op jit(solution)/shard_map/ppermute | solution.py:497
  66.2 1.4 %shard_map.219.sib = bf16[3456,256]{1,0:T(8,128)(2,1)S(1)} custom-call(bf16[3456,256]{1,0:T(8,128)(2,1)} %collective-permute-done.1.refs_0_), custom_call_target="tpu_custom_call" | custom-call | tf_op jit(solution)/shard_map/pallas_call | solution.py:616
  68.2 12.3 %all-to-all-done.2 = bf16[64,8,384]{2,1,0:T(8,128)(2,1)S(1)} async-done(((bf16[64,8,384]{2,1,0:T(8,128)(2,1)}), bf16[64,8,384]{2,1,0:T(8,128)(2,1)S(1)}, u32[]{:S(2)}, u32[]{:S(2)}) %all-to-all-start.2) | async-done | bytes 393248 | tf_op jit(solution)/shard_map/all_to_all | solution.py:493
  80.4 3.4 %shard_map.221 = bf16[512,384]{1,0:T(8,128)(2,1)} custom-call(bf16[512,384]{1,0:T(8,128)(2,1)S(1)} %bitcast.16, bf16[3456,256]{1,0:T(8,128)(2,1)} %shard_map.218.own_hbm, bf16[3456,256]{1,0:T(8,128)(2,1)S(1)} %shard_map.219.sib, bf16[288,1024]{1,0:T(8,128)(2,1)S(1)} %shard_map.220.dense_own, bf16[288,1024]{1,0:T(8,128)(2,1)S(1)} %collective-permute-done.5.dense_sib), custom_call_target="tpu_custom_call" | custom-call | tf_op jit(solution)/shard_map/pallas_call | solution.py:619
  83.9 5.0 %all-to-all-start.3 = ((bf16[64,8,384]{2,1,0:T(8,128)(2,1)}), bf16[64,8,384]{2,1,0:T(8,128)(2,1)S(1)}, u32[]{:S(2)}, u32[]{:S(2)}) async-start(bf16[64,8,384]{2,1,0:T(8,128)(2,1)} %bitcast.22), calls=%async_computation.3 | async-start | bytes 786432 | tf_op jit(solution)/shard_map/all_to_all | solution.py:493
  89.6 15.1 %all-to-all-done.3 = bf16[64,8,384]{2,1,0:T(8,128)(2,1)S(1)} async-done(((bf16[64,8,384]{2,1,0:T(8,128)(2,1)}), bf16[64,8,384]{2,1,0:T(8,128)(2,1)S(1)}, u32[]{:S(2)}, u32[]{:S(2)}) %all-to-all-start.3) | async-done | bytes 393248 | tf_op jit(solution)/shard_map/all_to_all | solution.py:493
  104.8 1.0 shard_map.222
  105.7 4.2 %all-to-all-start.4 = ((bf16[4,32,128]{2,1,0:T(8,128)(2,1)}), bf16[4,32,128]{2,1,0:T(8,128)(2,1)S(1)}, u32[]{:S(2)}, u32[]{:S(2)}) async-start(bf16[4,32,128]{2,1,0:T(8,128)(2,1)} %bitcast.14), calls=%async_computation.4 | async-start | bytes 65536 | tf_op jit(solution)/shard_map/all_to_all | solution.py:493
  109.9 0.8 shard_map.224
  110.7 4.7 %all-to-all-done.4.parts = bf16[4,32,128]{2,1,0:T(8,128)(2,1)S(1)} async-done(((bf16[4,32,128]{2,1,0:T(8,128)(2,1)}), bf16[4,32,128]{2,1,0:T(8,128)(2,1)S(1)}, u32[]{:S(2)}, u32[]{:S(2)}) %all-to-all-start.4) | async-done | bytes 32800 | tf_op jit(solution)/shard_map/all_to_all | solution.py:493
  115.4 0.6 shard_map.223
  (33 shorter events, 1.4 us)
Async XLA Ops:
  22.3 4.4 %copy-start.6 = (bf16[4,1032,128]{2,1,0:T(8,128)(2,1)}, bf16[4,1032,128]{2,1,0:T(8,128)(2,1)S(1)}, u32[]{:S(2)}) copy-start(bf16[4,1032,128]{2,1,0:T(8,128)(2,1)S(1)} %all_to_all.25.own_hbm) | copy-start | bytes 3170308
  22.3 8.9 %collective-permute-start = (bf16[4,1032,128]{2,1,0:T(8,128)(2,1)S(1)}, bf16[4,1032,128]{2,1,0:T(8,128)(2,1)S(1)}, u32[]{:S(2)}, u32[]{:S(2)}) collective-permute-start(bf16[4,1032,128]{2,1,0:T(8,128)(2,1)S(1)} %all_to_all.25.own_hbm), channel_id=1, source_target_pairs={{0,4},{4,0},{1,5},{5,1},{2,6},{6,2},{3,7},{7,3},{8,12},{12,8},{9,1... | collective-permute-start | bytes 3170312 | tf_op jit(solution)/shard_map/ppermute | solution.py:497
  24.2 4.9 %copy-start.8 = (bf16[1024]{0:T(1024)(128)(2,1)S(1)}, bf16[1024]{0:T(1024)(128)(2,1)}, u32[]{:S(2)}) copy-start(bf16[1024]{0:T(1024)(128)(2,1)} %param.21) | copy-start | bytes 6148
  24.2 4.9 %copy-start.9 = (bf16[1024]{0:T(1024)(128)(2,1)S(1)}, bf16[1024]{0:T(1024)(128)(2,1)}, u32[]{:S(2)}) copy-start(bf16[1024]{0:T(1024)(128)(2,1)} %param.22) | copy-start | bytes 6148
  24.2 4.9 %copy-start.2 = (bf16[4,1024]{1,0:T(4,128)(2,1)S(1)}, bf16[4,1024]{1,0:T(4,128)(2,1)}, u32[]{:S(2)}) copy-start(bf16[4,1024]{1,0:T(4,128)(2,1)} %tokens.3) | copy-start | bytes 24580
  26.7 39.5 %collective-permute-start.1 = (bf16[3456,256]{1,0:T(8,128)(2,1)}, bf16[3456,256]{1,0:T(8,128)(2,1)}, u32[]{:S(2)}, u32[]{:S(2)}) collective-permute-start(bf16[3456,256]{1,0:T(8,128)(2,1)} %shard_map.218.own_hbm), channel_id=1, source_target_pairs={{0,4},{4,0},{1,5},{5,1},{2,6},{6,2},{3,7},{7,3},{8,12},{12,8},{9,1... | collective-permute-start | bytes 5308424 | tf_op jit(solution)/shard_map/ppermute | solution.py:497
  29.3 2.0 %copy-start.4 = (s32[4]{0:T(128)S(1)}, s32[4]{0:T(128)}, u32[]{:S(2)}) copy-start(s32[4]{0:T(128)} %lengths.1) | copy-start | bytes 52
  29.3 2.0 %copy-start.5 = (f32[8]{0:T(128)S(1)}, f32[8]{0:T(128)}, u32[]{:S(2)}) copy-start(f32[8]{0:T(128)} %param.27) | copy-start | bytes 100
  31.3 6.1 %copy-start.7 = (bf16[96,1024]{1,0:T(8,128)(2,1)S(1)}, bf16[96,1024]{1,0:T(8,128)(2,1)}, u32[]{:S(2)}) copy-start(bf16[96,1024]{1,0:T(8,128)(2,1)} %get-tuple-element.22.dense) | copy-start | bytes 589828
  34.1 12.9 %all-to-all-start.1 = ((bf16[4,32,128]{2,1,0:T(8,128)(2,1)}), bf16[4,32,128]{2,1,0:T(8,128)(2,1)S(1)}, u32[]{:S(2)}, u32[]{:S(2)}) async-start(bf16[4,32,128]{2,1,0:T(8,128)(2,1)} %get-tuple-element.20), calls=%async_computation.1 | async-start | bytes 65536 | tf_op jit(solution)/shard_map/all_to_all | solution.py:493
  37.3 26.8 %collective-permute-start.2 = (bf16[96,1024]{1,0:T(8,128)(2,1)S(1)}, bf16[96,1024]{1,0:T(8,128)(2,1)S(1)}, u32[]{:S(2)}, u32[]{:S(2)}) collective-permute-start(bf16[96,1024]{1,0:T(8,128)(2,1)S(1)} %copy-done.7), channel_id=1, source_target_pairs={{0,8},{8,0},{16,24},{24,16},{32,40},{40,32},{48,56},{56,48},{1,9},... | collective-permute-start | bytes 589832 | tf_op jit(solution)/shard_map/ppermute | solution.py:497
  40.0 24.2 %collective-permute-start.3 = (bf16[96,1024]{1,0:T(8,128)(2,1)S(1)}, bf16[96,1024]{1,0:T(8,128)(2,1)S(1)}, u32[]{:S(2)}, u32[]{:S(2)}) collective-permute-start(bf16[96,1024]{1,0:T(8,128)(2,1)S(1)} %copy-done.7), channel_id=1, source_target_pairs={{0,64},{64,0},{128,192},{192,128},{256,320},{320,256},{384,448},{4... | collective-permute-start | bytes 589832 | tf_op jit(solution)/shard_map/ppermute | solution.py:497
  44.0 20.2 %collective-permute-start.4 = (bf16[96,1024]{1,0:T(8,128)(2,1)S(1)}, bf16[96,1024]{1,0:T(8,128)(2,1)S(1)}, u32[]{:S(2)}, u32[]{:S(2)}) collective-permute-start(bf16[96,1024]{1,0:T(8,128)(2,1)S(1)} %copy-done.7), channel_id=1, source_target_pairs={{0,72},{8,64},{16,88},{24,80},{32,104},{40,96},{48,120},{56,112},{... | collective-permute-start | bytes 589832 | tf_op jit(solution)/shard_map/ppermute | solution.py:552
  47.9 32.5 %all-to-all-start.2 = ((bf16[64,8,384]{2,1,0:T(8,128)(2,1)}), bf16[64,8,384]{2,1,0:T(8,128)(2,1)S(1)}, u32[]{:S(2)}, u32[]{:S(2)}) async-start(bf16[64,8,384]{2,1,0:T(8,128)(2,1)} %bitcast.21), calls=%async_computation.2 | async-start | bytes 786432 | tf_op jit(solution)/shard_map/all_to_all | solution.py:493
  64.3 3.9 %collective-permute-start.5 = (bf16[288,1024]{1,0:T(8,128)(2,1)S(1)}, bf16[288,1024]{1,0:T(8,128)(2,1)S(1)}, u32[]{:S(2)}, u32[]{:S(2)}) collective-permute-start(bf16[288,1024]{1,0:T(8,128)(2,1)S(1)} %shard_map.220.dense_own), channel_id=1, source_target_pairs={{0,4},{4,0},{1,5},{5,1},{2,6},{6,2},{3,7},{7,3},{8,12},{12,8},{9,1... | collective-permute-start | bytes 1769480 | tf_op jit(solution)/shard_map/ppermute | solution.py:497
  80.4 8.4 %copy-start.3 = (bf16[1024]{0:T(1024)(128)(2,1)S(1)}, bf16[1024]{0:T(1024)(128)(2,1)}, u32[]{:S(2)}) copy-start(bf16[1024]{0:T(1024)(128)(2,1)} %param.34) | copy-start | bytes 6148
  83.9 20.9 %all-to-all-start.3 = ((bf16[64,8,384]{2,1,0:T(8,128)(2,1)}), bf16[64,8,384]{2,1,0:T(8,128)(2,1)S(1)}, u32[]{:S(2)}, u32[]{:S(2)}) async-start(bf16[64,8,384]{2,1,0:T(8,128)(2,1)} %bitcast.22), calls=%async_computation.3 | async-start | bytes 786432 | tf_op jit(solution)/shard_map/all_to_all | solution.py:493
  89.2 20.7 %copy-start = (bf16[1024,128]{1,0:T(8,128)(2,1)S(1)}, bf16[1024,128]{1,0:T(8,128)(2,1)}, u32[]{:S(2)}) copy-start(bf16[1024,128]{1,0:T(8,128)(2,1)} %wk.1) | copy-start | bytes 786436
  89.2 20.7 %copy-start.1 = (bf16[1024,128]{1,0:T(8,128)(2,1)S(1)}, bf16[1024,128]{1,0:T(8,128)(2,1)}, u32[]{:S(2)}) copy-start(bf16[1024,128]{1,0:T(8,128)(2,1)} %wv.1) | copy-start | bytes 786436
  105.7 9.6 %all-to-all-start.4 = ((bf16[4,32,128]{2,1,0:T(8,128)(2,1)}), bf16[4,32,128]{2,1,0:T(8,128)(2,1)S(1)}, u32[]{:S(2)}, u32[]{:S(2)}) async-start(bf16[4,32,128]{2,1,0:T(8,128)(2,1)} %bitcast.14), calls=%async_computation.4 | async-start | bytes 65536 | tf_op jit(solution)/shard_map/all_to_all | solution.py:493

commit v5 on v4

--- a/solution.py
+++ b/solution.py
@@ -153,26 +153,6 @@
 def join_kernel(a, b, c, out):
     for n, ref in enumerate((a, b, c)):
         out[DENSE_ROWS * n : DENSE_ROWS * (n + 1), :] = ref[...]
-
-
-def fetch_kernel(*refs):
-    n = (len(refs) - 1) // 2
-    sems = refs[-1]
-    copies = []
-    for k in range(n):
-        rows = refs[k].shape[0]
-        step = rows // 4
-        for q in range(4):
-            part = slice(q * step, (q + 1) * step)
-            copies.append(
-                pltpu.make_async_copy(
-                    refs[k].at[part, :], refs[n + k].at[part, :], sems.at[k, q]
-                )
-            )
-    for c in copies:
-        c.start()
-    for c in copies:
-        c.wait()
 
 
 def attend_kernel(
@@ -612,10 +592,6 @@
         weigh_kernel, shape(2, SLOTS, TOK, ROWS), [SMEM, VMEM, VMEM], limit=8
     )(tp, info, mix)
     received = a2a(rows.reshape(CHIPS, MSG, WIDE), ("z", "y"))
-    sources = (expert_sib,)
-    fetched = call(
-        fetch_kernel, (pltpu.VMEM((PACK, 256), BF16),), [HBM], [pltpu.SemaphoreType.DMA((1, 4))]
-    )(*(in_hbm(a) for a in sources))
     outs = call(
         expert_kernel,
         pltpu.HBM((ROWS, WIDE), BF16),
@@ -627,7 +603,7 @@
         ],
         16,
         HBM,
-    )(received.reshape(ROWS, WIDE), in_hbm(expert_own), *(in_vmem(a) for a in (*fetched, dense_three, dense_three_sib)))
+    )(received.reshape(ROWS, WIDE), in_hbm(expert_own), *(in_vmem(a) for a in (expert_sib, dense_three, dense_three_sib)))
     returned = a2a(outs.reshape(CHIPS, MSG, WIDE), ("z", "y"))
     partial = call(combine_kernel, shape(TOK, 128), [VMEM] * 2)(
         combine, returned.reshape(ROWS, WIDE)

time: 117 us -> 117 us (level)
  Pallas kernels: 18.4 us -> 16.9 us
  waiting for transfers between devices: 32.6 us -> 34.1 us
    ppermute x5, waiting for transfers between devices: 0.51 us -> 1.98 us  [swap(): lax.ppermute(array, axis, [(i, i ^ 1) for i in range(lax.axis_size(axis))])]
    pallas_call x1 -> x0, Pallas kernels: 1.45 us -> none  [body(): call(fetch_kernel, (pltpu.VMEM((PACK, 256), BF16),), [HBM], [pltpu.Semaph...]
  transfers between devices with their start and end apart: 10 -> 10, of which waited for: 4 -> 4; matrix products, arithmetic and copies ran while one was open for 0% -> 0% of each run, Pallas kernels for 10% -> 8%
where the time goes in v5:
time: 117 us; the launch traced here: 116 us
  starting transfers between devices  44.5 us (38%)
  waiting for transfers between devices  34.1 us (29%)
  blocking collectives  19.8 us (17%)
  Pallas kernels  16.9 us (14%)
    all_to_all x4, waiting for transfers between devices, a2a(): return lax.all_to_all(array, axis, split_axis=0, concat_axis=0, tiled=True)  32.1 us
    all_to_all x4, starting transfers between devices, a2a(): return lax.all_to_all(array, axis, split_axis=0, concat_axis=0, tiled=True)  28.7 us
    all_to_all x1, blocking collectives, a2a(): return lax.all_to_all(array, axis, split_axis=0, concat_axis=0, tiled=True)  19.8 us
    ppermute x5, starting transfers between devices, swap(): lax.ppermute(array, axis, [(i, i ^ 1) for i in range(lax.axis_size(axis))])  12.9 us
    pallas_call x1, Pallas kernels, body(): call(expert_kernel, pltpu.HBM((ROWS, WIDE), BF16), [VMEM, HBM] + [VMEM] *...  3.4 us
    ppermute x1, starting transfers between devices, body(): dense_v = lax.ppermute(dense_own, ('z', 'y'), both)  2.93 us
    pallas_call x1, Pallas kernels, body(): call(attend_kernel, (shape(OWN, D), shape(TP, 32, 128)), [SMEM, SMEM] + [...  2.81 us
    pallas_call x1, Pallas kernels, body(): call(expert_pack_kernel, pltpu.HBM((PACK, 256), BF16), [HBM] * 4, [pltpu....  2.42 us
  transfers between devices with their start and end apart: 10, of which 4 were waited for; matrix products, arithmetic and copies ran while one was open for 0% of the time, Pallas kernels for 8%

profile of v5, /device:TPU:8, one launch (start us, length us, event | category | flops | bytes accessed | tf_op | source)
XLA Modules:
  0.0 116.2 jit_solution(989413906900781662)
XLA Ops:
  0.6 2.2 %shard_map.212 = (bf16[4,1032,128]{2,1,0:T(8,128)(2,1)}, bf16[96,1024]{1,0:T(8,128)(2,1)}) custom-call(s32[1]{0:T(128)} %bitcast.core, bf16[1024,128]{1,0:T(8,128)(2,1)} %wq.1, bf16[128,1024]{1,0:T(8,128)(2,1)} %wo.1, s32[2,4]{1,0:T(2,128)} %bitcast.26, f32[2,4]{1,0:T(2,128)} %bitcast.27, bf16[32,1024]{1,0:T(8,128)(2,1)} %gate.1, bf16[32,1024]{1,0:T(8,128)(2,1)} %up.1, ...), custom_call_target="tpu_custom_call" | custom-call | tf_op jit(solution)/shard_map/pallas_call | solution.py:505
  2.8 19.8 %all_to_all.25.own_hbm = bf16[4,1032,128]{2,1,0:T(8,128)(2,1)} all-to-all(bf16[4,1032,128]{2,1,0:T(8,128)(2,1)} %get-tuple-element.14), channel_id=1, replica_groups=mesh['z'=8,'y'=8,'c'=2,'x'=4] {'x'}, dimensions={0} | all-to-all | bytes 2113536 | tf_op jit(solution)/shard_map/all_to_all | solution.py:473
  22.6 1.9 %collective-permute-start = (bf16[4,1032,128]{2,1,0:T(8,128)(2,1)}, bf16[4,1032,128]{2,1,0:T(8,128)(2,1)S(1)}, u32[]{:S(2)}, u32[]{:S(2)}) collective-permute-start(bf16[4,1032,128]{2,1,0:T(8,128)(2,1)} %all_to_all.25.own_hbm), channel_id=1, source_target_pairs={{0,4},{4,0},{1,5},{5,1},{2,6},{6,2},{3,7},{7,3},{8,12},{12,8},{9,1... | collective-permute-start | bytes 3170312 | tf_op jit(solution)/shard_map/ppermute | solution.py:477
  24.6 2.4 %shard_map.218.own_hbm = bf16[3456,256]{1,0:T(8,128)(2,1)} custom-call(bf16[1024,256]{1,0:T(8,128)(2,1)} %bitcast.23, bf16[1024,256]{1,0:T(8,128)(2,1)} %bitcast.24, bf16[256,1024]{1,0:T(8,128)(2,1)} %bitcast.25, bf16[96,1024]{1,0:T(8,128)(2,1)} %get-tuple-element.22.dense), custom_call_target="tpu_custom_call" | custom-call | tf_op jit(solution)/shard_map/pallas_call | solution.py:534
  27.0 2.4 %collective-permute-start.1 = (bf16[3456,256]{1,0:T(8,128)(2,1)}, bf16[3456,256]{1,0:T(8,128)(2,1)S(1)}, u32[]{:S(2)}, u32[]{:S(2)}) collective-permute-start(bf16[3456,256]{1,0:T(8,128)(2,1)} %shard_map.218.own_hbm), channel_id=1, source_target_pairs={{0,4},{4,0},{1,5},{5,1},{2,6},{6,2},{3,7},{7,3},{8,12},{12,8},{9,1... | collective-permute-start | bytes 5308424 | tf_op jit(solution)/shard_map/ppermute | solution.py:477
  29.6 2.0 %shard_map.213 = (bf16[3,512,128]{2,1,0:T(8,128)(2,1)S(1)}, f32[128,128]{1,0:T(8,128)S(1)}, bf16[4,1032,128]{2,1,0:T(8,128)(2,1)S(1)}, bf16[4,1024,128]{2,1,0:T(8,128)(2,1)S(1)}, bf16[4,1024,128]{2,1,0:T(8,128)(2,1)S(1)}) custom-call(s32[1]{0:T(128)} %bitcast.1.tp, bf16[4,1032,128]{2,1,0:T(8,128)(2,1)} %all_to_all.25.own_hbm, ...), custom_call_target="tpu_custom_call" | custom-call | tf_op jit(solution)/shard_map/pallas_call | solution.py:553
  31.6 2.8 %shard_map.214 = (bf16[4,1024]{1,0:T(4,128)(2,1)S(1)}, bf16[4,32,128]{2,1,0:T(8,128)(2,1)}) custom-call(s32[1]{0:T(128)} %bitcast.core, s32[4]{0:T(128)S(1)} %copy-done.4, bf16[4,1024]{1,0:T(4,128)(2,1)S(1)} %copy-done.2, bf16[4,1024]{1,0:T(4,128)(2,1)S(1)} %shard_map.211.attn_in, bf16[4,1032,128]{2,1,0:T(8,128)(2,1)S(1)} %get-tuple-element.15.w_own, ...), custom_call_target="tpu_custom_call" | custom-call | tf_op jit(solution)/shard_map/pallas_call | solution.py:565
  34.4 3.3 %all-to-all-start.1 = ((bf16[4,32,128]{2,1,0:T(8,128)(2,1)}), bf16[4,32,128]{2,1,0:T(8,128)(2,1)S(1)}, u32[]{:S(2)}, u32[]{:S(2)}) async-start(bf16[4,32,128]{2,1,0:T(8,128)(2,1)} %get-tuple-element.20), calls=%async_computation.1 | async-start | bytes 65536 | tf_op jit(solution)/shard_map/all_to_all | solution.py:473
  37.6 3.2 %collective-permute-start.2 = (bf16[96,1024]{1,0:T(8,128)(2,1)}, bf16[96,1024]{1,0:T(8,128)(2,1)S(1)}, u32[]{:S(2)}, u32[]{:S(2)}) collective-permute-start(bf16[96,1024]{1,0:T(8,128)(2,1)} %get-tuple-element.22.dense), channel_id=1, source_target_pairs={{0,8},{8,0},{16,24},{24,16},{32,40},{40,32},{48,56},{56,48},{1,9},... | collective-permute-start | bytes 589832 | tf_op jit(solution)/shard_map/ppermute | solution.py:477
  40.8 3.5 %collective-permute-start.3 = (bf16[96,1024]{1,0:T(8,128)(2,1)}, bf16[96,1024]{1,0:T(8,128)(2,1)S(1)}, u32[]{:S(2)}, u32[]{:S(2)}) collective-permute-start(bf16[96,1024]{1,0:T(8,128)(2,1)} %get-tuple-element.22.dense), channel_id=1, source_target_pairs={{0,64},{64,0},{128,192},{192,128},{256,320},{320,256},{384,448},{4... | collective-permute-start | bytes 589832 | tf_op jit(solution)/shard_map/ppermute | solution.py:477
  44.3 2.9 %collective-permute-start.4 = (bf16[96,1024]{1,0:T(8,128)(2,1)}, bf16[96,1024]{1,0:T(8,128)(2,1)S(1)}, u32[]{:S(2)}, u32[]{:S(2)}) collective-permute-start(bf16[96,1024]{1,0:T(8,128)(2,1)} %get-tuple-element.22.dense), channel_id=1, source_target_pairs={{0,72},{8,64},{16,88},{24,80},{32,104},{40,96},{48,120},{56,112},{... | collective-permute-start | bytes 589832 | tf_op jit(solution)/shard_map/ppermute | solution.py:532
  47.2 1.0 shard_map.217
  48.2 16.2 %all-to-all-start.2 = ((bf16[64,8,384]{2,1,0:T(8,128)(2,1)}), bf16[64,8,384]{2,1,0:T(8,128)(2,1)S(1)}, u32[]{:S(2)}, u32[]{:S(2)}) async-start(bf16[64,8,384]{2,1,0:T(8,128)(2,1)} %bitcast.21), calls=%async_computation.2 | async-start | bytes 786432 | tf_op jit(solution)/shard_map/all_to_all | solution.py:473
  64.5 1.9 %collective-permute-start.5 = (bf16[288,1024]{1,0:T(8,128)(2,1)S(1)}, bf16[288,1024]{1,0:T(8,128)(2,1)S(1)}, u32[]{:S(2)}, u32[]{:S(2)}) collective-permute-start(bf16[288,1024]{1,0:T(8,128)(2,1)S(1)} %shard_map.219.dense_own), channel_id=1, source_target_pairs={{0,4},{4,0},{1,5},{5,1},{2,6},{6,2},{3,7},{7,3},{8,12},{12,8},{9,1... | collective-permute-start | bytes 1769480 | tf_op jit(solution)/shard_map/ppermute | solution.py:477
  66.5 2.0 %collective-permute-done.5.dense_sib = bf16[288,1024]{1,0:T(8,128)(2,1)S(1)} collective-permute-done((bf16[288,1024]{1,0:T(8,128)(2,1)S(1)}, bf16[288,1024]{1,0:T(8,128)(2,1)S(1)}, u32[]{:S(2)}, u32[]{:S(2)}) %collective-permute-start.5) | collective-permute-done | bytes 589856 | tf_op jit(solution)/shard_map/ppermute | solution.py:477
  68.4 12.3 %all-to-all-done.2 = bf16[64,8,384]{2,1,0:T(8,128)(2,1)S(1)} async-done(((bf16[64,8,384]{2,1,0:T(8,128)(2,1)}), bf16[64,8,384]{2,1,0:T(8,128)(2,1)S(1)}, u32[]{:S(2)}, u32[]{:S(2)}) %all-to-all-start.2) | async-done | bytes 393248 | tf_op jit(solution)/shard_map/all_to_all | solution.py:473
  80.7 3.4 %shard_map.220 = bf16[512,384]{1,0:T(8,128)(2,1)} custom-call(bf16[512,384]{1,0:T(8,128)(2,1)S(1)} %bitcast.16, bf16[3456,256]{1,0:T(8,128)(2,1)} %shard_map.218.own_hbm, bf16[3456,256]{1,0:T(8,128)(2,1)S(1)} %collective-permute-done.1.sib, bf16[288,1024]{1,0:T(8,128)(2,1)S(1)} %shard_map.219.dense_own, bf16[288,1024]{1,0:T(8,128)(2,1)S(1)} %collective-permute-done.5.dense_sib), custom_call_target="tpu_custom_call" | custom-call | tf_op jit(solution)/shard_map/pallas_call | solution.py:595
  84.1 5.0 %all-to-all-start.3 = ((bf16[64,8,384]{2,1,0:T(8,128)(2,1)}), bf16[64,8,384]{2,1,0:T(8,128)(2,1)S(1)}, u32[]{:S(2)}, u32[]{:S(2)}) async-start(bf16[64,8,384]{2,1,0:T(8,128)(2,1)} %bitcast.22), calls=%async_computation.3 | async-start | bytes 786432 | tf_op jit(solution)/shard_map/all_to_all | solution.py:473
  89.9 15.1 %all-to-all-done.3 = bf16[64,8,384]{2,1,0:T(8,128)(2,1)S(1)} async-done(((bf16[64,8,384]{2,1,0:T(8,128)(2,1)}), bf16[64,8,384]{2,1,0:T(8,128)(2,1)S(1)}, u32[]{:S(2)}, u32[]{:S(2)}) %all-to-all-start.3) | async-done | bytes 393248 | tf_op jit(solution)/shard_map/all_to_all | solution.py:473
  105.0 1.0 shard_map.221
  106.0 4.2 %all-to-all-start.4 = ((bf16[4,32,128]{2,1,0:T(8,128)(2,1)}), bf16[4,32,128]{2,1,0:T(8,128)(2,1)S(1)}, u32[]{:S(2)}, u32[]{:S(2)}) async-start(bf16[4,32,128]{2,1,0:T(8,128)(2,1)} %bitcast.14), calls=%async_computation.4 | async-start | bytes 65536 | tf_op jit(solution)/shard_map/all_to_all | solution.py:473
  110.2 0.8 shard_map.223
  110.9 4.7 %all-to-all-done.4.parts = bf16[4,32,128]{2,1,0:T(8,128)(2,1)S(1)} async-done(((bf16[4,32,128]{2,1,0:T(8,128)(2,1)}), bf16[4,32,128]{2,1,0:T(8,128)(2,1)S(1)}, u32[]{:S(2)}, u32[]{:S(2)}) %all-to-all-start.4) | async-done | bytes 32800 | tf_op jit(solution)/shard_map/all_to_all | solution.py:473
  115.6 0.6 shard_map.222
  (28 shorter events, 0.9 us)
Async XLA Ops:
  22.6 8.9 %collective-permute-start = (bf16[4,1032,128]{2,1,0:T(8,128)(2,1)}, bf16[4,1032,128]{2,1,0:T(8,128)(2,1)S(1)}, u32[]{:S(2)}, u32[]{:S(2)}) collective-permute-start(bf16[4,1032,128]{2,1,0:T(8,128)(2,1)} %all_to_all.25.own_hbm), channel_id=1, source_target_pairs={{0,4},{4,0},{1,5},{5,1},{2,6},{6,2},{3,7},{7,3},{8,12},{12,8},{9,1... | collective-permute-start | bytes 3170312 | tf_op jit(solution)/shard_map/ppermute | solution.py:477
  24.5 4.9 %copy-start.6 = (bf16[1024]{0:T(1024)(128)(2,1)S(1)}, bf16[1024]{0:T(1024)(128)(2,1)}, u32[]{:S(2)}) copy-start(bf16[1024]{0:T(1024)(128)(2,1)} %param.21) | copy-start | bytes 6148
  24.5 4.9 %copy-start.7 = (bf16[1024]{0:T(1024)(128)(2,1)S(1)}, bf16[1024]{0:T(1024)(128)(2,1)}, u32[]{:S(2)}) copy-start(bf16[1024]{0:T(1024)(128)(2,1)} %param.22) | copy-start | bytes 6148
  24.5 4.9 %copy-start.2 = (bf16[4,1024]{1,0:T(4,128)(2,1)S(1)}, bf16[4,1024]{1,0:T(4,128)(2,1)}, u32[]{:S(2)}) copy-start(bf16[4,1024]{1,0:T(4,128)(2,1)} %tokens.3) | copy-start | bytes 24580
  27.0 41.5 %collective-permute-start.1 = (bf16[3456,256]{1,0:T(8,128)(2,1)}, bf16[3456,256]{1,0:T(8,128)(2,1)S(1)}, u32[]{:S(2)}, u32[]{:S(2)}) collective-permute-start(bf16[3456,256]{1,0:T(8,128)(2,1)} %shard_map.218.own_hbm), channel_id=1, source_target_pairs={{0,4},{4,0},{1,5},{5,1},{2,6},{6,2},{3,7},{7,3},{8,12},{12,8},{9,1... | collective-permute-start | bytes 5308424 | tf_op jit(solution)/shard_map/ppermute | solution.py:477
  29.6 2.0 %copy-start.4 = (s32[4]{0:T(128)S(1)}, s32[4]{0:T(128)}, u32[]{:S(2)}) copy-start(s32[4]{0:T(128)} %lengths.1) | copy-start | bytes 52
  29.6 2.0 %copy-start.5 = (f32[8]{0:T(128)S(1)}, f32[8]{0:T(128)}, u32[]{:S(2)}) copy-start(f32[8]{0:T(128)} %param.27) | copy-start | bytes 100
  34.4 12.9 %all-to-all-start.1 = ((bf16[4,32,128]{2,1,0:T(8,128)(2,1)}), bf16[4,32,128]{2,1,0:T(8,128)(2,1)S(1)}, u32[]{:S(2)}, u32[]{:S(2)}) async-start(bf16[4,32,128]{2,1,0:T(8,128)(2,1)} %get-tuple-element.20), calls=%async_computation.1 | async-start | bytes 65536 | tf_op jit(solution)/shard_map/all_to_all | solution.py:473
  37.6 26.8 %collective-permute-start.2 = (bf16[96,1024]{1,0:T(8,128)(2,1)}, bf16[96,1024]{1,0:T(8,128)(2,1)S(1)}, u32[]{:S(2)}, u32[]{:S(2)}) collective-permute-start(bf16[96,1024]{1,0:T(8,128)(2,1)} %get-tuple-element.22.dense), channel_id=1, source_target_pairs={{0,8},{8,0},{16,24},{24,16},{32,40},{40,32},{48,56},{56,48},{1,9},... | collective-permute-start | bytes 589832 | tf_op jit(solution)/shard_map/ppermute | solution.py:477
  40.8 23.7 %collective-permute-start.3 = (bf16[96,1024]{1,0:T(8,128)(2,1)}, bf16[96,1024]{1,0:T(8,128)(2,1)S(1)}, u32[]{:S(2)}, u32[]{:S(2)}) collective-permute-start(bf16[96,1024]{1,0:T(8,128)(2,1)} %get-tuple-element.22.dense), channel_id=1, source_target_pairs={{0,64},{64,0},{128,192},{192,128},{256,320},{320,256},{384,448},{4... | collective-permute-start | bytes 589832 | tf_op jit(solution)/shard_map/ppermute | solution.py:477
  44.3 20.2 %collective-permute-start.4 = (bf16[96,1024]{1,0:T(8,128)(2,1)}, bf16[96,1024]{1,0:T(8,128)(2,1)S(1)}, u32[]{:S(2)}, u32[]{:S(2)}) collective-permute-start(bf16[96,1024]{1,0:T(8,128)(2,1)} %get-tuple-element.22.dense), channel_id=1, source_target_pairs={{0,72},{8,64},{16,88},{24,80},{32,104},{40,96},{48,120},{56,112},{... | collective-permute-start | bytes 589832 | tf_op jit(solution)/shard_map/ppermute | solution.py:532
  48.2 32.5 %all-to-all-start.2 = ((bf16[64,8,384]{2,1,0:T(8,128)(2,1)}), bf16[64,8,384]{2,1,0:T(8,128)(2,1)S(1)}, u32[]{:S(2)}, u32[]{:S(2)}) async-start(bf16[64,8,384]{2,1,0:T(8,128)(2,1)} %bitcast.21), calls=%async_computation.2 | async-start | bytes 786432 | tf_op jit(solution)/shard_map/all_to_all | solution.py:473
  64.5 3.9 %collective-permute-start.5 = (bf16[288,1024]{1,0:T(8,128)(2,1)S(1)}, bf16[288,1024]{1,0:T(8,128)(2,1)S(1)}, u32[]{:S(2)}, u32[]{:S(2)}) collective-permute-start(bf16[288,1024]{1,0:T(8,128)(2,1)S(1)} %shard_map.219.dense_own), channel_id=1, source_target_pairs={{0,4},{4,0},{1,5},{5,1},{2,6},{6,2},{3,7},{7,3},{8,12},{12,8},{9,1... | collective-permute-start | bytes 1769480 | tf_op jit(solution)/shard_map/ppermute | solution.py:477
  80.7 8.4 %copy-start.3 = (bf16[1024]{0:T(1024)(128)(2,1)S(1)}, bf16[1024]{0:T(1024)(128)(2,1)}, u32[]{:S(2)}) copy-start(bf16[1024]{0:T(1024)(128)(2,1)} %param.34) | copy-start | bytes 6148
  84.1 20.9 %all-to-all-start.3 = ((bf16[64,8,384]{2,1,0:T(8,128)(2,1)}), bf16[64,8,384]{2,1,0:T(8,128)(2,1)S(1)}, u32[]{:S(2)}, u32[]{:S(2)}) async-start(bf16[64,8,384]{2,1,0:T(8,128)(2,1)} %bitcast.22), calls=%async_computation.3 | async-start | bytes 786432 | tf_op jit(solution)/shard_map/all_to_all | solution.py:473
  89.4 20.8 %copy-start = (bf16[1024,128]{1,0:T(8,128)(2,1)S(1)}, bf16[1024,128]{1,0:T(8,128)(2,1)}, u32[]{:S(2)}) copy-start(bf16[1024,128]{1,0:T(8,128)(2,1)} %wk.1) | copy-start | bytes 786436
  89.4 20.7 %copy-start.1 = (bf16[1024,128]{1,0:T(8,128)(2,1)S(1)}, bf16[1024,128]{1,0:T(8,128)(2,1)}, u32[]{:S(2)}) copy-start(bf16[1024,128]{1,0:T(8,128)(2,1)} %wv.1) | copy-start | bytes 786436
  106.0 9.6 %all-to-all-start.4 = ((bf16[4,32,128]{2,1,0:T(8,128)(2,1)}), bf16[4,32,128]{2,1,0:T(8,128)(2,1)S(1)}, u32[]{:S(2)}, u32[]{:S(2)}) async-start(bf16[4,32,128]{2,1,0:T(8,128)(2,1)} %bitcast.14), calls=%async_computation.4 | async-start | bytes 65536 | tf_op jit(solution)/shard_map/all_to_all | solution.py:473
